TPU v7x, 256 devices: a whole 4x4x8 slice. The times are simulated.
256 devices in a mesh: sp: 128 (over z, y, x), tp: 2 (over core).
Axes of the slice: x: 4, y: 4, z: 8, core: 2. Of those that a mesh axis runs over, the one named last changes fastest.
Arguments:
- stream: bfloat16 [57344, 2048], P('sp'), may hold values from -6 to 6
- norm_gain: float32 [2, 2048], replicated, may hold values from 0.1 to 1.9
- value_weight: bfloat16 [2, 2048, 512], P(None, None, 'tp'), may hold values from -0.125 to 0.125
- gate_weight: bfloat16 [2, 2048, 512], P(None, None, 'tp'), may hold values from -0.125 to 0.125
- conv_taps: bfloat16 [2, 512, 512], P(None, None, 'tp'), may hold values from -0.25 to 0.25
- conv_bias: float32 [2, 512], P(None, 'tp'), may hold values from -3 to 3
- channel_gain: float32 [2, 512], replicated, may hold values from 0.1 to 1.9
- channel_shift: float32 [2, 512], replicated, may hold values from -3 to 3
- out_weight: bfloat16 [2, 512, 2048], replicated, may hold values from -0.25 to 0.25
Outputs:
- result: bfloat16 [57344, 2048], P('sp')
All inputs are finite; a program needn't handle non-finite values.
Results may differ from a plain program's by a relative error of at most 0.0075.
Values may be sent and summed in bfloat16 or wider, within the bound.
A program may use at most 64 MiB of HBM per device.

v0:
```python
import jax
import jax.numpy as jnp
from jax import lax
from jax.sharding import PartitionSpec as P


def passed_along(value, axis, by):
    count = lax.axis_size(axis)
    pairs = [(i, i + by) for i in range(count) if 0 <= i + by < count]
    return lax.ppermute(value, axis, pairs)


def rms_normed(stream, gain):
    values = stream.astype(jnp.float32)
    scale = lax.rsqrt(jnp.mean(values * values, axis=-1, keepdims=True) + 1e-06)
    return (values * scale * gain[None, :]).astype(jnp.bfloat16)


def channel_mix(conv, gain, shift):
    values = conv.astype(jnp.float32)
    center = jnp.mean(values, axis=-1, keepdims=True)
    spread = jnp.mean(jnp.square(values - center), axis=-1, keepdims=True)
    normed = (values - center) * lax.rsqrt(spread + 1e-05) * gain[None, :] + shift[None, :]
    return jax.nn.silu(normed).astype(jnp.bfloat16)


def gate_rows(normed, w_value, w_gate):
    values = jnp.dot(normed, w_value, preferred_element_type=jnp.float32)
    gates = jnp.dot(normed, w_gate, preferred_element_type=jnp.float32)
    return (values * jax.nn.sigmoid(gates)).astype(jnp.bfloat16)


def per_device(
    stream,
    norm_gain,
    value_weight,
    gate_weight,
    conv_taps,
    conv_bias,
    channel_gain,
    channel_shift,
    out_weight,
):
    tokens = stream.shape[0]
    reach = conv_taps.shape[1] - 1
    hops = -(-reach // tokens)
    state = stream
    for layer in range(norm_gain.shape[0]):
        normed = rms_normed(state, norm_gain[layer])
        own_gated = gate_rows(normed, value_weight[layer], gate_weight[layer])
        pieces = [own_gated]
        for step in range(1, hops + 1):
            count = min(tokens, reach - (step - 1) * tokens)
            pieces.insert(0, passed_along(own_gated[tokens - count :], "sp", step))
        gated = jnp.concatenate(pieces, axis=0)
        conv = lax.conv_general_dilated(
            gated[None],
            conv_taps[layer][:, None, :],
            (1,),
            [(0, 0)],
            dimension_numbers=("NWC", "WIO", "NWC"),
            feature_group_count=gated.shape[1],
            preferred_element_type=jnp.float32,
        )[0]
        conv = (conv + conv_bias[layer][None, :]).astype(jnp.bfloat16)
        every_channel = lax.all_gather(conv, "tp", axis=1, tiled=True)
        mixed = channel_mix(every_channel, channel_gain[layer], channel_shift[layer])
        update = jnp.dot(mixed, out_weight[layer], preferred_element_type=jnp.float32)
        state = (state.astype(jnp.float32) + update).astype(jnp.bfloat16)
    return state


def solution(mesh):
    return jax.shard_map(
        per_device,
        mesh=mesh,
        in_specs=(
            P("sp", None),
            P(),
            P(None, None, "tp"),
            P(None, None, "tp"),
            P(None, None, "tp"),
            P(None, "tp"),
            P(),
            P(),
            P(),
        ),
        out_specs=P("sp", None),
        check_vma=False,
    )
```

profile of v0, /device:TPU:129, one launch (start us, length us, event | category | flops | bytes accessed | tf_op | source)
XLA Modules:
  0.0 102.5 jit_solution(44458553434053622)
XLA Ops:
  0.0 1.9 %fusion = f32[448]{0:T(512)S(1)} fusion(bf16[448,2048]{1,0:T(8,128)(2,1)} %param.9), kind=kLoop, calls=%fused_computation.6 | loop fusion | flops 2752064 | bytes 1836800 | tf_op jit(solution)/shard_map/reduce_sum | solution.py:15
  1.9 0.8 fusion.76
  2.8 0.0 copy-start
  2.8 0.0 copy-start.7
  2.8 2.6 %fusion.17 = f32[448,256]{1,0:T(8,128)S(1)} fusion(bf16[2,2048,256]{2,1,0:T(8,128)(2,1)} %param.12, bf16[448,2048]{1,0:T(8,128)(2,1)} %param.9, f32[2048]{0:T(1024)S(1)} %bitcast.46, f32[448]{0:T(512)S(1)} %add_rsqrt_fusion.3), kind=kOutput, calls=%fused_computation.27 | convolution fusion | flops 473776128 | bytes 3352320 | tf_op jit(solution)/shard_map/dot_general | solution.py:29
  5.4 0.3 copy-done.7
  5.8 0.7 fusion.18
  6.5 3.1 %collective-permute-start.1 = (bf16[448,256]{1,0:T(8,128)(2,1)S(1)}, bf16[448,256]{1,0:T(8,128)(2,1)S(1)}, u32[]{:S(2)}, u32[]{:S(2)}) collective-permute-start(bf16[448,256]{1,0:T(8,128)(2,1)S(1)} %fusion.18), channel_id=1, source_target_pairs={{0,2},{2,4},{4,6},{6,8},{8,10},{10,12},{12,14},{14,16},{16,18},{18... | collective-permute-start | bytes 688136 | tf_op jit(solution)/shard_map/ppermute | solution.py:10
  9.7 4.4 %collective-permute-start = (bf16[63,256]{1,0:T(8,128)(2,1)S(1)}, bf16[63,256]{1,0:T(8,128)(2,1)S(1)}, u32[]{:S(2)}, u32[]{:S(2)}) collective-permute-start(bf16[63,256]{1,0:T(8,128)(2,1)S(1)} %slice.72), channel_id=1, source_target_pairs={{0,4},{2,6},{4,8},{6,10},{8,12},{10,14},{12,16},{14,18},{16,20},{1... | collective-permute-start | bytes 96776 | tf_op jit(solution)/shard_map/ppermute | solution.py:10
  14.1 0.0 copy-done.3
  14.2 6.3 %collective-permute-done = bf16[63,256]{1,0:T(8,128)(2,1)S(1)} collective-permute-done((bf16[63,256]{1,0:T(8,128)(2,1)S(1)}, bf16[63,256]{1,0:T(8,128)(2,1)S(1)}, u32[]{:S(2)}, u32[]{:S(2)}) %collective-permute-start) | collective-permute-done | bytes 32288 | tf_op jit(solution)/shard_map/ppermute | solution.py:10
  20.4 0.0 collective-permute-done.1
  20.4 0.1 maximum_bitcast_fusion
  20.6 0.0 copy-start.5
  20.6 26.7 %fusion.34 = f32[1,448,256]{2,0,1:T(1,128)S(1)} fusion(bf16[1,959,256]{2,1,0:T(8,128)(2,1)S(1)} %maximum_bitcast_fusion, bf16[512,1,256]{2,0,1:T(8,128)(2,1)S(1)} %get-tuple-element.6), kind=kOutput, calls=%fused_computation.48 | convolution fusion | flops 117440512 | bytes 1211904 | tf_op jit(solution)/shard_map/conv_general_dilated | solution.py:56
  47.3 3.9 %all_gather.6 = bf16[448,512]{1,0:T(8,128)(2,1)S(1)} all-gather(bf16[448,256]{1,0:T(8,128)(2,1)S(1)} %fusion.63), channel_id=1, replica_groups=mesh['sp'=128,'tp'=2] {'tp'}, dimensions={1}, use_global_device_ids=true | all-gather | bytes 688128 | tf_op jit(solution)/shard_map/all_gather | solution.py:66
  51.2 0.1 convert_reduce_fusion.1
  51.4 0.3 fusion.45
  51.7 0.0 copy-start.6
  51.7 1.7 %fusion.4 = (f32[448]{0:T(512)S(1)}, bf16[448,2048]{1,0:T(8,128)(2,1)S(1)}) fusion(bf16[2,512,2048]{2,1,0:T(8,128)(2,1)S(1)} %copy-done.5, bf16[448,512]{1,0:T(8,128)(2,1)S(1)} %all_gather.6, f32[512]{0:T(512)S(1)} %bitcast.53, f32[512]{0:T(512)S(1)} %bitcast.52, f32[448]{0:T(512)S(1)} %add_rsqrt_fusion.2, f32[448]{0:T(512)S(1)} %broadcast_multiply_fusion.1, ...), kind=kOutput, calls=%fused_computation.10 | convolution fusion | flops 947322432 | bytes 6235904 | tf_op jit(solution)/shard_map/dot_general | solution.py:68
  53.4 0.7 fusion.14
  54.1 0.7 fusion.19
  54.8 2.7 %collective-permute-start.3 = (bf16[448,256]{1,0:T(8,128)(2,1)S(1)}, bf16[448,256]{1,0:T(8,128)(2,1)S(1)}, u32[]{:S(2)}, u32[]{:S(2)}) collective-permute-start(bf16[448,256]{1,0:T(8,128)(2,1)S(1)} %fusion.19), channel_id=1, source_target_pairs={{0,2},{2,4},{4,6},{6,8},{8,10},{10,12},{12,14},{14,16},{16,18},{18... | collective-permute-start | bytes 688136 | tf_op jit(solution)/shard_map/ppermute | solution.py:10
  57.5 1.9 %collective-permute-start.2 = (bf16[63,256]{1,0:T(8,128)(2,1)S(1)}, bf16[63,256]{1,0:T(8,128)(2,1)S(1)}, u32[]{:S(2)}, u32[]{:S(2)}) collective-permute-start(bf16[63,256]{1,0:T(8,128)(2,1)S(1)} %slice.73), channel_id=1, source_target_pairs={{0,4},{2,6},{4,8},{6,10},{8,12},{10,14},{12,16},{14,18},{16,20},{1... | collective-permute-start | bytes 96776 | tf_op jit(solution)/shard_map/ppermute | solution.py:10
  59.5 8.8 %collective-permute-done.2 = bf16[63,256]{1,0:T(8,128)(2,1)S(1)} collective-permute-done((bf16[63,256]{1,0:T(8,128)(2,1)S(1)}, bf16[63,256]{1,0:T(8,128)(2,1)S(1)}, u32[]{:S(2)}, u32[]{:S(2)}) %collective-permute-start.2) | collective-permute-done | bytes 32288 | tf_op jit(solution)/shard_map/ppermute | solution.py:10
  68.3 0.7 collective-permute-done.3
  69.0 0.1 maximum_bitcast_fusion.1
  69.1 26.6 %fusion.32 = f32[1,448,256]{2,0,1:T(1,128)S(1)} fusion(bf16[1,959,256]{2,1,0:T(8,128)(2,1)S(1)} %maximum_bitcast_fusion.1, bf16[512,1,256]{2,0,1:T(8,128)(2,1)S(1)} %get-tuple-element.5), kind=kOutput, calls=%fused_computation.46 | convolution fusion | flops 117440512 | bytes 1211904 | tf_op jit(solution)/shard_map/conv_general_dilated | solution.py:56
  95.8 3.6 %all_gather.7 = bf16[448,512]{1,0:T(8,128)(2,1)S(1)} all-gather(bf16[448,256]{1,0:T(8,128)(2,1)S(1)} %fusion.62), channel_id=1, replica_groups=mesh['sp'=128,'tp'=2] {'tp'}, dimensions={1}, use_global_device_ids=true | all-gather | bytes 688128 | tf_op jit(solution)/shard_map/all_gather | solution.py:66
  99.4 0.1 convert_reduce_fusion
  99.6 0.3 fusion.36
  99.9 2.6 %fusion.7 = bf16[448,2048]{1,0:T(8,128)(2,1)} fusion(bf16[448,2048]{1,0:T(8,128)(2,1)S(1)} %get-tuple-element.16, bf16[2,512,2048]{2,1,0:T(8,128)(2,1)S(1)} %copy-done.5, bf16[448,512]{1,0:T(8,128)(2,1)S(1)} %all_gather.7, f32[512]{0:T(512)S(1)} %bitcast.51, f32[512]{0:T(512)S(1)} %bitcast.50, f32[448]{0:T(512)S(1)} %add_rsqrt_fusion, ...), kind=kOutput, calls=%fused_computation.13 | convolution fusion | flops 944570368 | bytes 6234112 | tf_op jit(solution)/shard_map/dot_general | solution.py:68
  (24 shorter events, 0.2 us)
Async XLA Ops:
  2.8 2.7 %copy-start = (bf16[448,2048]{1,0:T(8,128)(2,1)S(1)}, bf16[448,2048]{1,0:T(8,128)(2,1)}, u32[]{:S(2)}) copy-start(bf16[448,2048]{1,0:T(8,128)(2,1)} %param.9) | copy-start | bytes 5505028
  2.8 3.0 %copy-start.7 = (bf16[2,2048,256]{2,1,0:T(8,128)(2,1)S(1)}, bf16[2,2048,256]{2,1,0:T(8,128)(2,1)}, u32[]{:S(2)}) copy-start(bf16[2,2048,256]{2,1,0:T(8,128)(2,1)} %param.11) | copy-start | bytes 6291460
  5.8 8.2 %copy-start.2 = (f32[2,512]{1,0:T(2,128)S(1)}, f32[2,512]{1,0:T(2,128)}, u32[]{:S(2)}) copy-start(f32[2,512]{1,0:T(2,128)} %param.15) | copy-start | bytes 12292
  5.8 8.3 %copy-start.1 = (bf16[2,512,256]{2,1,0:T(8,128)(2,1)S(1)}, bf16[2,512,256]{2,1,0:T(8,128)(2,1)}, u32[]{:S(2)}) copy-start(bf16[2,512,256]{2,1,0:T(8,128)(2,1)} %param.13) | copy-start | bytes 1572868
  5.8 8.3 %copy-start.3 = (f32[2,512]{1,0:T(2,128)S(1)}, f32[2,512]{1,0:T(2,128)}, u32[]{:S(2)}) copy-start(f32[2,512]{1,0:T(2,128)} %param.16) | copy-start | bytes 12292
  5.8 8.3 %copy-start.4 = (f32[2,256]{1,0:T(2,128)S(1)}, f32[2,256]{1,0:T(2,128)}, u32[]{:S(2)}) copy-start(f32[2,256]{1,0:T(2,128)} %param.14) | copy-start | bytes 6148
  6.5 13.9 %collective-permute-start.1 = (bf16[448,256]{1,0:T(8,128)(2,1)S(1)}, bf16[448,256]{1,0:T(8,128)(2,1)S(1)}, u32[]{:S(2)}, u32[]{:S(2)}) collective-permute-start(bf16[448,256]{1,0:T(8,128)(2,1)S(1)} %fusion.18), channel_id=1, source_target_pairs={{0,2},{2,4},{4,6},{6,8},{8,10},{10,12},{12,14},{14,16},{16,18},{18... | collective-permute-start | bytes 688136 | tf_op jit(solution)/shard_map/ppermute | solution.py:10
  9.7 10.8 %collective-permute-start = (bf16[63,256]{1,0:T(8,128)(2,1)S(1)}, bf16[63,256]{1,0:T(8,128)(2,1)S(1)}, u32[]{:S(2)}, u32[]{:S(2)}) collective-permute-start(bf16[63,256]{1,0:T(8,128)(2,1)S(1)} %slice.72), channel_id=1, source_target_pairs={{0,4},{2,6},{4,8},{6,10},{8,12},{10,14},{12,16},{14,18},{16,20},{1... | collective-permute-start | bytes 96776 | tf_op jit(solution)/shard_map/ppermute | solution.py:10
  20.6 31.1 %copy-start.5 = (bf16[2,512,2048]{2,1,0:T(8,128)(2,1)S(1)}, bf16[2,512,2048]{2,1,0:T(8,128)(2,1)}, u32[]{:S(2)}) copy-start(bf16[2,512,2048]{2,1,0:T(8,128)(2,1)} %param.17) | copy-start | bytes 12582916
  51.7 1.7 %copy-start.6 = (bf16[2,2048,256]{2,1,0:T(8,128)(2,1)S(1)}, bf16[2,2048,256]{2,1,0:T(8,128)(2,1)}, u32[]{:S(2)}) copy-start(bf16[2,2048,256]{2,1,0:T(8,128)(2,1)} %param.12) | copy-start | bytes 6291460
  54.8 14.2 %collective-permute-start.3 = (bf16[448,256]{1,0:T(8,128)(2,1)S(1)}, bf16[448,256]{1,0:T(8,128)(2,1)S(1)}, u32[]{:S(2)}, u32[]{:S(2)}) collective-permute-start(bf16[448,256]{1,0:T(8,128)(2,1)S(1)} %fusion.19), channel_id=1, source_target_pairs={{0,2},{2,4},{4,6},{6,8},{8,10},{10,12},{12,14},{14,16},{16,18},{18... | collective-permute-start | bytes 688136 | tf_op jit(solution)/shard_map/ppermute | solution.py:10
  57.5 10.7 %collective-permute-start.2 = (bf16[63,256]{1,0:T(8,128)(2,1)S(1)}, bf16[63,256]{1,0:T(8,128)(2,1)S(1)}, u32[]{:S(2)}, u32[]{:S(2)}) collective-permute-start(bf16[63,256]{1,0:T(8,128)(2,1)S(1)} %slice.73), channel_id=1, source_target_pairs={{0,4},{2,6},{4,8},{6,10},{8,12},{10,14},{12,16},{14,18},{16,20},{1... | collective-permute-start | bytes 96776 | tf_op jit(solution)/shard_map/ppermute | solution.py:10
where the time goes:
time: 103 us
  matrix products  62.4 us (61%)
  waiting for transfers between devices  15.8 us (15%)
  starting transfers between devices  12.1 us (12%)
  blocking collectives  7.49 us (7%)
  other arithmetic  3.19 us (3%)
  local copies, waits for them, and re-layouts  1.27 us (1%)
    conv_general_dilated x2, matrix products, per_device(): lax.conv_general_dilated(gated[None], conv_taps[layer][:, None, :], (1,),...  53.3 us
    ppermute x4, waiting for transfers between devices, passed_along(): return lax.ppermute(value, axis, pairs)  15.8 us
    ppermute x4, starting transfers between devices, passed_along(): return lax.ppermute(value, axis, pairs)  12.1 us
    all_gather x2, blocking collectives, per_device(): every_channel = lax.all_gather(conv, 'tp', axis=1, tiled=True)  7.49 us
    dot_general x2, matrix products, per_device(): jnp.dot(mixed, out_weight[layer], preferred_element_type=jnp.float32)  4.28 us
    dot_general x2, matrix products, gate_rows(): gates = jnp.dot(normed, w_gate, preferred_element_type=jnp.float32)  3.36 us
  transfers between devices with their start and end apart: 4, of which 3 were waited for; matrix products, arithmetic and copies ran while one was open for 0% of the time, Pallas kernels for 0%

commit v1 on v0

--- a/solution.py
+++ b/solution.py
@@ -1,7 +1,57 @@
 import jax
 import jax.numpy as jnp
+import numpy as np
 from jax import lax
 from jax.sharding import PartitionSpec as P
+
+BLOCK = 128
+BF16 = jnp.bfloat16
+
+
+def halves(matrix):
+    high = matrix.astype(np.float32).astype(BF16)
+    low = (matrix - high.astype(np.float64)).astype(np.float32).astype(BF16)
+    return high, low
+
+
+def spectra():
+    odd = 2 * np.arange(BLOCK)[:, None] + 1
+    n = np.arange(BLOCK)[None, :]
+    angle = np.pi * odd * n / (2 * BLOCK)
+    forward = np.concatenate([np.cos(angle), -np.sin(angle)])
+    reverse = forward[:, ::-1]
+    angle = angle + np.pi * odd / 2
+    inverse = np.concatenate([np.cos(angle), -np.sin(angle)]).T / BLOCK
+    return forward, reverse, inverse
+
+
+def two_pass(matrix, blocks):
+    high, low = halves(matrix)
+    one = lambda m: jnp.einsum("fn,bnc->bfc", jnp.asarray(m), blocks, preferred_element_type=jnp.float32)
+    return one(high) + one(low)
+
+
+def causal_conv(window, taps):
+    forward, reverse, inverse = spectra()
+    channels = window.shape[1]
+    signal = two_pass(forward, window.reshape(-1, BLOCK, channels))
+    lags = two_pass(reverse, taps.reshape(-1, BLOCK, channels))[::-1]
+    sign = jnp.asarray(np.where(np.arange(BLOCK) % 2, -1.0, 1.0).astype(np.float32))[None, :, None]
+    re, im = lags[:, :BLOCK], lags[:, BLOCK:]
+    turned_re, turned_im = sign * im, -sign * re
+    zero = jnp.zeros_like(re[:1])
+    h_re = jnp.concatenate([turned_re, zero]) + jnp.concatenate([zero, re])
+    h_im = jnp.concatenate([turned_im, zero]) + jnp.concatenate([zero, im])
+    a_re, a_im = signal[:, :BLOCK], signal[:, BLOCK:]
+    count = signal.shape[0] - 4
+    y_re = sum(h_re[c] * a_re[4 - c : 4 - c + count] - h_im[c] * a_im[4 - c : 4 - c + count] for c in range(5))
+    y_im = sum(h_re[c] * a_im[4 - c : 4 - c + count] + h_im[c] * a_re[4 - c : 4 - c + count] for c in range(5))
+    y = jnp.concatenate([y_re, y_im], axis=1)
+    y_high = y.astype(BF16)
+    y_low = (y - y_high.astype(jnp.float32)).astype(BF16)
+    high, low = halves(inverse)
+    one = lambda m, v: jnp.einsum("nf,bfc->bnc", jnp.asarray(m), v, preferred_element_type=jnp.float32)
+    return (one(high, y_high) + one(high, y_low) + one(low, y_high)).reshape(-1, channels)
 
 
 def passed_along(value, axis, by):
@@ -42,7 +92,7 @@
     out_weight,
 ):
     tokens = stream.shape[0]
-    reach = conv_taps.shape[1] - 1
+    reach = conv_taps.shape[1]
     hops = -(-reach // tokens)
     state = stream
     for layer in range(norm_gain.shape[0]):
@@ -52,16 +102,9 @@
         for step in range(1, hops + 1):
             count = min(tokens, reach - (step - 1) * tokens)
             pieces.insert(0, passed_along(own_gated[tokens - count :], "sp", step))
-        gated = jnp.concatenate(pieces, axis=0)
-        conv = lax.conv_general_dilated(
-            gated[None],
-            conv_taps[layer][:, None, :],
-            (1,),
-            [(0, 0)],
-            dimension_numbers=("NWC", "WIO", "NWC"),
-            feature_group_count=gated.shape[1],
-            preferred_element_type=jnp.float32,
-        )[0]
+        pieces.append(jnp.zeros((-(reach + tokens) % BLOCK, own_gated.shape[1]), own_gated.dtype))
+        window = jnp.concatenate(pieces, axis=0)
+        conv = causal_conv(window, conv_taps[layer])[:tokens]
         conv = (conv + conv_bias[layer][None, :]).astype(jnp.bfloat16)
         every_channel = lax.all_gather(conv, "tp", axis=1, tiled=True)
         mixed = channel_mix(every_channel, channel_gain[layer], channel_shift[layer])

time: 103 us -> 61 us (0.59)
  matrix products: 62.4 us -> 14.8 us
  waiting for transfers between devices: 15.8 us -> 7.29 us
  local copies, waits for them, and re-layouts: 1.27 us -> 9.32 us
  other arithmetic: 3.19 us -> 6.91 us
  starting transfers between devices: 12.1 us -> 14.3 us
    conv_general_dilated x2 -> x0, matrix products: 53.3 us -> none  [per_device(): lax.conv_general_dilated(gated[None], conv_taps[layer][:, None, :], (1,),...]
    ppermute x4, waiting for transfers between devices: 15.8 us -> 7.29 us  [passed_along(): return lax.ppermute(value, axis, pairs)]
    dot_general x0 -> x14, matrix products: none -> 5.05 us  [the longest x8 3.65 us: two_pass(): jnp.einsum('fn,bnc->bfc', jnp.asarray(m), blocks, preferred_element_type=...]
    unnamed x16 -> x54, local copies, waits for them, and re-layouts: 0.38 us -> 3.89 us
    ppermute x4, starting transfers between devices: 12.1 us -> 14.3 us  [passed_along(): return lax.ppermute(value, axis, pairs)]
    slice x0 -> x7, local copies, waits for them, and re-layouts: none -> 1.99 us  [the longest x6 1.95 us: causal_conv(): re, im = (lags[:, :BLOCK], lags[:, BLOCK:])]
    concatenate x0 -> x2, other arithmetic: none -> 1.45 us  [per_device(): window = jnp.concatenate(pieces, axis=0)]
    slice x2, local copies, waits for them, and re-layouts: 0.02 us -> 1.39 us  [per_device(): pieces.insert(0, passed_along(own_gated[tokens - count:], 'sp', step))]
  transfers between devices with their start and end apart: 4 -> 4, of which waited for: 3 -> 2; matrix products, arithmetic and copies ran while one was open for 0% -> 11% of each run, Pallas kernels for 0% -> 0%
where the time goes in v1:
time: 61 us; the launch traced here: 60.4 us
  matrix products  14.8 us (24%)
  starting transfers between devices  14.3 us (23%)
  local copies, waits for them, and re-layouts  9.32 us (15%)
  waiting for transfers between devices  7.29 us (12%)
  blocking collectives  7.23 us (12%)
  other arithmetic  6.91 us (11%)
    ppermute x4, starting transfers between devices, passed_along(): return lax.ppermute(value, axis, pairs)  14.3 us
    ppermute x4, waiting for transfers between devices, passed_along(): return lax.ppermute(value, axis, pairs)  7.29 us
    all_gather x2, blocking collectives, per_device(): every_channel = lax.all_gather(conv, 'tp', axis=1, tiled=True)  7.23 us
    dot_general x2, matrix products, per_device(): jnp.dot(mixed, out_weight[layer], preferred_element_type=jnp.float32)  4.28 us
    unnamed x54, local copies, waits for them, and re-layouts  3.89 us
    dot_general x8, matrix products, two_pass(): jnp.einsum('fn,bnc->bfc', jnp.asarray(m), blocks, preferred_element_type=...  3.65 us
    dot_general x2, matrix products, gate_rows(): gates = jnp.dot(normed, w_gate, preferred_element_type=jnp.float32)  3.35 us
    dot_general x2, matrix products, gate_rows(): values = jnp.dot(normed, w_value, preferred_element_type=jnp.float32)  2.12 us
  transfers between devices with their start and end apart: 4, of which 2 were waited for; matrix products, arithmetic and copies ran while one was open for 11% of the time, Pallas kernels for 0%

profile of v1, /device:TPU:129, one launch (start us, length us, event | category | flops | bytes accessed | tf_op | source)
XLA Modules:
  0.0 60.4 jit_solution(4755459158372254712)
XLA Ops:
  0.0 1.9 %fusion = f32[448]{0:T(512)S(1)} fusion(bf16[448,2048]{1,0:T(8,128)(2,1)} %param.23), kind=kLoop, calls=%fused_computation.6 | loop fusion | flops 2752064 | bytes 1836800 | tf_op jit(solution)/shard_map/reduce_sum | solution.py:65
  1.9 0.8 %fusion.127 = (f32[1,2048]{1,0:T(1,128)S(1)}, f32[1,2048]{1,0:T(1,128)S(1)}) fusion(f32[2,2048]{1,0:T(2,128)} %param.24), kind=kLoop, calls=%fused_computation.195 | loop fusion | bytes 32768 | tf_op jit(solution)/shard_map/slice | solution.py:99
  2.8 2.6 %fusion.19 = f32[448,256]{1,0:T(8,128)S(1)} fusion(bf16[2,2048,256]{2,1,0:T(8,128)(2,1)} %param.26, bf16[448,2048]{1,0:T(8,128)(2,1)} %param.23, f32[2048]{0:T(1024)S(1)} %bitcast.126, f32[448]{0:T(512)S(1)} %add_rsqrt_fusion.3), kind=kOutput, calls=%fused_computation.37 | convolution fusion | flops 473776128 | bytes 3352320 | tf_op jit(solution)/shard_map/dot_general | solution.py:79
  5.4 0.3 copy-done.25
  5.8 1.4 %fusion.20 = bf16[448,256]{1,0:T(8,128)(2,1)} fusion(f32[448,256]{1,0:T(8,128)S(1)} %fusion.19, bf16[2,2048,256]{2,1,0:T(8,128)(2,1)S(1)} %copy-done.25, bf16[448,2048]{1,0:T(8,128)(2,1)S(1)} %copy-done.2, f32[2048]{0:T(1024)S(1)} %bitcast.127, f32[448]{0:T(512)S(1)} %add_rsqrt_fusion.3), kind=kOutput, calls=%fused_computation.38 | convolution fusion | flops 473661440 | bytes 3581952 | tf_op jit(solution)/shard_map/dot_general | solution.py:78
  7.2 3.2 %collective-permute-start.1 = (bf16[448,256]{1,0:T(8,128)(2,1)}, bf16[448,256]{1,0:T(8,128)(2,1)}, u32[]{:S(2)}, u32[]{:S(2)}) collective-permute-start(bf16[448,256]{1,0:T(8,128)(2,1)} %fusion.20), channel_id=1, source_target_pairs={{0,2},{2,4},{4,6},{6,8},{8,10},{10,12},{12,14},{14,16},{16,18},{18... | collective-permute-start | bytes 688136 | tf_op jit(solution)/shard_map/ppermute | solution.py:60
  10.5 1.4 %slice.340 = bf16[64,256]{1,0:T(8,128)(2,1)} slice(bf16[448,256]{1,0:T(8,128)(2,1)} %fusion.20), slice={[384:448], [0:256]} | slice | bytes 65536 | tf_op jit(solution)/shard_map/slice | solution.py:104
  11.8 4.3 %collective-permute-start = (bf16[64,256]{1,0:T(8,128)(2,1)}, bf16[64,256]{1,0:T(8,128)(2,1)}, u32[]{:S(2)}, u32[]{:S(2)}) collective-permute-start(bf16[64,256]{1,0:T(8,128)(2,1)} %slice.340), channel_id=1, source_target_pairs={{0,4},{2,6},{4,8},{6,10},{8,12},{10,14},{12,16},{14,18},{16,20},{1... | collective-permute-start | bytes 98312 | tf_op jit(solution)/shard_map/ppermute | solution.py:60
  16.2 0.6 fusion.128
  16.8 0.6 fusion.129
  18.1 0.8 %slice.272 = f32[4,128,256]{2,1,0:T(8,128)} reverse(f32[4,128,256]{2,1,0:T(8,128)S(1)} %get-tuple-element.27), dimensions={0} | reverse | bytes 1048576 | tf_op jit(solution)/shard_map/slice | solution.py:40
  19.0 0.8 %slice.270 = f32[4,128,256]{2,1,0:T(8,128)} reverse(f32[4,128,256]{2,1,0:T(8,128)S(1)} %get-tuple-element.28), dimensions={0} | reverse | bytes 1048576 | tf_op jit(solution)/shard_map/slice | solution.py:40
  21.0 0.8 %copy-done.1 = f32[4,128,256]{2,1,0:T(8,128)S(1)} copy-done((f32[4,128,256]{2,1,0:T(8,128)S(1)}, f32[4,128,256]{2,1,0:T(8,128)}, u32[]{:S(2)}) %copy-start.1) | copy-done | bytes 524312
  22.0 0.8 %fusion.83 = (f32[128,256]{1,0:T(8,128)S(1)}, f32[128,256]{1,0:T(8,128)S(1)}, f32[128,256]{1,0:T(8,128)}, f32[128,256]{1,0:T(8,128)}, f32[128,256]{1,0:T(8,128)}) fusion(f32[4,128,256]{2,1,0:T(8,128)S(1)} %get-tuple-element.45, f32[4,128,256]{2,1,0:T(8,128)S(1)} %copy-done), kind=kLoop, calls=%fused_computation.141 | loop fusion | flops 163840 | bytes 1703936 | tf_op jit(solution)/shard_map/mul | solution.py:47
  22.9 1.3 %maximum_maximum_fusion = bf16[1024,256]{1,0:T(8,128)(2,1)S(1)} fusion(bf16[448,256]{1,0:T(8,128)(2,1)} %fusion.20, bf16[448,256]{1,0:T(8,128)(2,1)} %collective-permute-done.1, bf16[64,256]{1,0:T(8,128)(2,1)} %collective-permute-done, bf16[1024]{0:T(1024)(128)(2,1)S(1)} %pad.19.clone), kind=kLoop, calls=%fused_computation.112 | loop fusion | flops 2097152 | bytes 1017856 | tf_op jit(solution)/shard_map/concatenate | solution.py:106
  24.2 1.3 %fusion.133 = f32[8,256,256]{1,2,0:T(8,128)S(1)} fusion(bf16[256,128,1]{1,0,2:T(8,128)(2,1)} %constant.65, bf16[8,128,256]{2,1,0:T(8,128)(2,1)S(1)} %bitcast.116), kind=kOutput, calls=%fused_computation.201 | convolution fusion | flops 134217728 | bytes 2686976 | tf_op jit(solution)/shard_map/fn,bnc->bfc/dot_general | solution.py:30
  25.5 0.4 add_bitcast_fusion.1
  25.9 0.4 copy-done.4
  27.2 0.5 copy-done.7
  28.1 0.3 copy-done.10
  28.8 3.6 %all_gather.6 = bf16[448,512]{1,0:T(8,128)(2,1)S(1)} all-gather(bf16[448,256]{1,0:T(8,128)(2,1)S(1)} %fusion.61), channel_id=1, replica_groups=mesh['sp'=128,'tp'=2] {'tp'}, dimensions={1}, use_global_device_ids=true | all-gather | bytes 688128 | tf_op jit(solution)/shard_map/all_gather | solution.py:109
  32.9 1.6 %fusion.4 = (f32[448]{0:T(512)S(1)}, bf16[448,2048]{1,0:T(8,128)(2,1)S(1)}) fusion(bf16[2,512,2048]{2,1,0:T(8,128)(2,1)S(1)} %copy-done.23, bf16[448,512]{1,0:T(8,128)(2,1)S(1)} %all_gather.6, f32[512]{0:T(512)S(1)} %bitcast.133, f32[512]{0:T(512)S(1)} %bitcast.132, f32[448]{0:T(512)S(1)} %add_rsqrt_fusion.2, f32[448]{0:T(512)S(1)} %broadcast_multiply_fusion.5, ...), kind=kOutput, calls=%fused_computation.10 | convolution fusion | flops 947322432 | bytes 6235904 | tf_op jit(solution)/shard_map/dot_general | solution.py:111
  34.6 0.7 %fusion.16 = f32[448,256]{1,0:T(8,128)S(1)} fusion(bf16[2,2048,256]{2,1,0:T(8,128)(2,1)S(1)} %copy-done.24, bf16[448,2048]{1,0:T(8,128)(2,1)S(1)} %get-tuple-element.44, f32[2048]{0:T(1024)S(1)} %bitcast.124, f32[448]{0:T(512)S(1)} %add_rsqrt_fusion.1), kind=kOutput, calls=%fused_computation.33 | convolution fusion | flops 473776128 | bytes 3352576 | tf_op jit(solution)/shard_map/dot_general | solution.py:79
  35.3 0.9 %copy-done.26 = bf16[2,2048,256]{2,1,0:T(8,128)(2,1)S(1)} copy-done((bf16[2,2048,256]{2,1,0:T(8,128)(2,1)S(1)}, bf16[2,2048,256]{2,1,0:T(8,128)(2,1)}, u32[]{:S(2)}) %copy-start.26) | copy-done | bytes 2097176
  36.2 0.7 %fusion.21 = bf16[448,256]{1,0:T(8,128)(2,1)S(1)} fusion(f32[448,256]{1,0:T(8,128)S(1)} %fusion.16, bf16[2,2048,256]{2,1,0:T(8,128)(2,1)S(1)} %copy-done.26, bf16[448,2048]{1,0:T(8,128)(2,1)S(1)} %get-tuple-element.44, f32[2048]{0:T(1024)S(1)} %bitcast.125, f32[448]{0:T(512)S(1)} %add_rsqrt_fusion.1), kind=kOutput, calls=%fused_computation.39 | convolution fusion | flops 473661440 | bytes 3581952 | tf_op jit(solution)/shard_map/dot_general | solution.py:78
  36.9 3.1 %collective-permute-start.3 = (bf16[448,256]{1,0:T(8,128)(2,1)S(1)}, bf16[448,256]{1,0:T(8,128)(2,1)S(1)}, u32[]{:S(2)}, u32[]{:S(2)}) collective-permute-start(bf16[448,256]{1,0:T(8,128)(2,1)S(1)} %fusion.21), channel_id=1, source_target_pairs={{0,2},{2,4},{4,6},{6,8},{8,10},{10,12},{12,14},{14,16},{16,18},{18... | collective-permute-start | bytes 688136 | tf_op jit(solution)/shard_map/ppermute | solution.py:60
  40.1 3.6 %collective-permute-start.2 = (bf16[64,256]{1,0:T(8,128)(2,1)S(1)}, bf16[64,256]{1,0:T(8,128)(2,1)S(1)}, u32[]{:S(2)}, u32[]{:S(2)}) collective-permute-start(bf16[64,256]{1,0:T(8,128)(2,1)S(1)} %slice.370), channel_id=1, source_target_pairs={{0,4},{2,6},{4,8},{6,10},{8,12},{10,14},{12,16},{14,18},{16,20},{1... | collective-permute-start | bytes 98312 | tf_op jit(solution)/shard_map/ppermute | solution.py:60
  43.8 7.1 %collective-permute-done.2 = bf16[64,256]{1,0:T(8,128)(2,1)S(1)} collective-permute-done((bf16[64,256]{1,0:T(8,128)(2,1)S(1)}, bf16[64,256]{1,0:T(8,128)(2,1)S(1)}, u32[]{:S(2)}, u32[]{:S(2)}) %collective-permute-start.2) | collective-permute-done | bytes 32800 | tf_op jit(solution)/shard_map/ppermute | solution.py:60
  51.3 0.4 fusion.134
  51.7 0.4 add_bitcast_fusion
  53.6 3.6 %all_gather.7 = bf16[448,512]{1,0:T(8,128)(2,1)S(1)} all-gather(bf16[448,256]{1,0:T(8,128)(2,1)S(1)} %fusion.60), channel_id=1, replica_groups=mesh['sp'=128,'tp'=2] {'tp'}, dimensions={1}, use_global_device_ids=true | all-gather | bytes 688128 | tf_op jit(solution)/shard_map/all_gather | solution.py:109
  57.7 2.6 %fusion.7 = bf16[448,2048]{1,0:T(8,128)(2,1)} fusion(bf16[448,2048]{1,0:T(8,128)(2,1)S(1)} %get-tuple-element.44, bf16[2,512,2048]{2,1,0:T(8,128)(2,1)S(1)} %copy-done.23, bf16[448,512]{1,0:T(8,128)(2,1)S(1)} %all_gather.7, f32[512]{0:T(512)S(1)} %bitcast.131, f32[512]{0:T(512)S(1)} %bitcast.130, f32[448]{0:T(512)S(1)} %add_rsqrt_fusion, ...), kind=kOutput, calls=%fused_computation.13 | convolution fusion | flops 944570368 | bytes 6234112 | tf_op jit(solution)/shard_map/dot_general | solution.py:111
  (91 shorter events, 6.7 us)
Async XLA Ops:
  2.8 2.7 %copy-start.2 = (bf16[448,2048]{1,0:T(8,128)(2,1)S(1)}, bf16[448,2048]{1,0:T(8,128)(2,1)}, u32[]{:S(2)}) copy-start(bf16[448,2048]{1,0:T(8,128)(2,1)} %param.23) | copy-start | bytes 5505028
  2.8 3.0 %copy-start.25 = (bf16[2,2048,256]{2,1,0:T(8,128)(2,1)S(1)}, bf16[2,2048,256]{2,1,0:T(8,128)(2,1)}, u32[]{:S(2)}) copy-start(bf16[2,2048,256]{2,1,0:T(8,128)(2,1)} %param.25) | copy-start | bytes 6291460
  5.8 10.4 %copy-start.16 = (f32[2,256]{1,0:T(2,128)S(1)}, f32[2,256]{1,0:T(2,128)}, u32[]{:S(2)}) copy-start(f32[2,256]{1,0:T(2,128)} %param.28) | copy-start | bytes 6148
  5.8 10.4 %copy-start.14 = (f32[2,512]{1,0:T(2,128)S(1)}, f32[2,512]{1,0:T(2,128)}, u32[]{:S(2)}) copy-start(f32[2,512]{1,0:T(2,128)} %param.29) | copy-start | bytes 12292
  5.8 11.0 %copy-start.15 = (f32[2,512]{1,0:T(2,128)S(1)}, f32[2,512]{1,0:T(2,128)}, u32[]{:S(2)}) copy-start(f32[2,512]{1,0:T(2,128)} %param.30) | copy-start | bytes 12292
  5.8 11.6 %copy-start.8 = (bf16[2,512,256]{2,1,0:T(8,128)(2,1)S(1)}, bf16[2,512,256]{2,1,0:T(8,128)(2,1)}, u32[]{:S(2)}) copy-start(bf16[2,512,256]{2,1,0:T(8,128)(2,1)} %param.27) | copy-start | bytes 1572868
  5.8 11.6 %copy-start.12 = (bf16[256,128,1]{1,0,2:T(8,128)(2,1)S(1)}, bf16[256,128,1]{1,0,2:T(8,128)(2,1)}, u32[]{:S(2)}) copy-start(bf16[256,128,1]{1,0,2:T(8,128)(2,1)} %constant.63) | copy-start | bytes 196612
  7.2 10.5 %copy-start.11 = (bf16[256,128,1]{1,0,2:T(8,128)(2,1)S(1)}, bf16[256,128,1]{1,0,2:T(8,128)(2,1)}, u32[]{:S(2)}) copy-start(bf16[256,128,1]{1,0,2:T(8,128)(2,1)} %constant.64) | copy-start | bytes 196612
  7.2 15.7 %collective-permute-start.1 = (bf16[448,256]{1,0:T(8,128)(2,1)}, bf16[448,256]{1,0:T(8,128)(2,1)}, u32[]{:S(2)}, u32[]{:S(2)}) collective-permute-start(bf16[448,256]{1,0:T(8,128)(2,1)} %fusion.20), channel_id=1, source_target_pairs={{0,2},{2,4},{4,6},{6,8},{8,10},{10,12},{12,14},{14,16},{16,18},{18... | collective-permute-start | bytes 688136 | tf_op jit(solution)/shard_map/ppermute | solution.py:60
  11.8 11.1 %collective-permute-start = (bf16[64,256]{1,0:T(8,128)(2,1)}, bf16[64,256]{1,0:T(8,128)(2,1)}, u32[]{:S(2)}, u32[]{:S(2)}) collective-permute-start(bf16[64,256]{1,0:T(8,128)(2,1)} %slice.340), channel_id=1, source_target_pairs={{0,4},{2,6},{4,8},{6,10},{8,12},{10,14},{12,16},{14,18},{16,20},{1... | collective-permute-start | bytes 98312 | tf_op jit(solution)/shard_map/ppermute | solution.py:60
  20.1 0.7 %copy-start.21 = (f32[128]{0:T(128)S(1)}, f32[128]{0:T(128)}, u32[]{:S(2)}) copy-start(f32[128]{0:T(128)} %constant.62) | copy-start | bytes 1540
  20.1 0.7 %copy-start.22 = (f32[128]{0:T(128)S(1)}, f32[128]{0:T(128)}, u32[]{:S(2)}) copy-start(f32[128]{0:T(128)} %constant.42.clone) | copy-start | bytes 1540
  20.8 1.0 %copy-start.1 = (f32[4,128,256]{2,1,0:T(8,128)S(1)}, f32[4,128,256]{2,1,0:T(8,128)}, u32[]{:S(2)}) copy-start(f32[4,128,256]{2,1,0:T(8,128)} %slice.270) | copy-start | bytes 1572868
  20.8 1.2 %copy-start = (f32[4,128,256]{2,1,0:T(8,128)S(1)}, f32[4,128,256]{2,1,0:T(8,128)}, u32[]{:S(2)}) copy-start(f32[4,128,256]{2,1,0:T(8,128)} %slice.272) | copy-start | bytes 1572868
  22.8 2.6 %copy-start.9 = (bf16[256,128,1]{1,0,2:T(8,128)(2,1)S(1)}, bf16[256,128,1]{1,0,2:T(8,128)(2,1)}, u32[]{:S(2)}) copy-start(bf16[256,128,1]{1,0,2:T(8,128)(2,1)} %constant.66) | copy-start | bytes 196612
  25.4 0.9 %copy-start.4 = (f32[128,256]{1,0:T(8,128)S(1)}, f32[128,256]{1,0:T(8,128)}, u32[]{:S(2)}) copy-start(f32[128,256]{1,0:T(8,128)} %get-tuple-element.19) | copy-start | bytes 393220
  25.5 1.0 %copy-start.5 = (f32[128,256]{1,0:T(8,128)S(1)}, f32[128,256]{1,0:T(8,128)}, u32[]{:S(2)}) copy-start(f32[128,256]{1,0:T(8,128)} %get-tuple-element.20) | copy-start | bytes 393220
  25.5 1.0 %copy-start.6 = (f32[128,256]{1,0:T(8,128)S(1)}, f32[128,256]{1,0:T(8,128)}, u32[]{:S(2)}) copy-start(f32[128,256]{1,0:T(8,128)} %get-tuple-element.21) | copy-start | bytes 393220
  26.8 0.8 %copy-start.7 = (bf16[128,256,1]{1,0,2:T(8,128)(2,1)S(1)}, bf16[128,256,1]{1,0,2:T(8,128)(2,1)}, u32[]{:S(2)}) copy-start(bf16[128,256,1]{1,0,2:T(8,128)(2,1)} %constant.67) | copy-start | bytes 196612
  27.7 0.8 %copy-start.10 = (bf16[128,256,1]{1,0,2:T(8,128)(2,1)S(1)}, bf16[128,256,1]{1,0,2:T(8,128)(2,1)}, u32[]{:S(2)}) copy-start(bf16[128,256,1]{1,0,2:T(8,128)(2,1)} %constant.68) | copy-start | bytes 196612
  27.9 5.0 %copy-start.23 = (bf16[2,512,2048]{2,1,0:T(8,128)(2,1)S(1)}, bf16[2,512,2048]{2,1,0:T(8,128)(2,1)}, u32[]{:S(2)}) copy-start(bf16[2,512,2048]{2,1,0:T(8,128)(2,1)} %param.31) | copy-start | bytes 12582916
  28.5 4.4 %copy-start.3 = (bf16[448,2048]{1,0:T(8,128)(2,1)S(1)}, bf16[448,2048]{1,0:T(8,128)(2,1)}, u32[]{:S(2)}) copy-start(bf16[448,2048]{1,0:T(8,128)(2,1)} %param.23) | copy-start | bytes 5505028
  28.5 4.4 %copy-start.19 = (f32[1,512]{1,0:T(1,128)S(1)}, f32[1,512]{1,0:T(1,128)}, u32[]{:S(2)}) copy-start(f32[1,512]{1,0:T(1,128)} %get-tuple-element.34) | copy-start | bytes 6148
  28.5 4.4 %copy-start.20 = (f32[1,512]{1,0:T(1,128)S(1)}, f32[1,512]{1,0:T(1,128)}, u32[]{:S(2)}) copy-start(f32[1,512]{1,0:T(1,128)} %get-tuple-element.36) | copy-start | bytes 6148
  32.9 1.7 %copy-start.24 = (bf16[2,2048,256]{2,1,0:T(8,128)(2,1)S(1)}, bf16[2,2048,256]{2,1,0:T(8,128)(2,1)}, u32[]{:S(2)}) copy-start(bf16[2,2048,256]{2,1,0:T(8,128)(2,1)} %param.26) | copy-start | bytes 6291460
  34.6 1.6 %copy-start.26 = (bf16[2,2048,256]{2,1,0:T(8,128)(2,1)S(1)}, bf16[2,2048,256]{2,1,0:T(8,128)(2,1)}, u32[]{:S(2)}) copy-start(bf16[2,2048,256]{2,1,0:T(8,128)(2,1)} %param.25) | copy-start | bytes 6291460
  36.9 14.2 %collective-permute-start.3 = (bf16[448,256]{1,0:T(8,128)(2,1)S(1)}, bf16[448,256]{1,0:T(8,128)(2,1)S(1)}, u32[]{:S(2)}, u32[]{:S(2)}) collective-permute-start(bf16[448,256]{1,0:T(8,128)(2,1)S(1)} %fusion.21), channel_id=1, source_target_pairs={{0,2},{2,4},{4,6},{6,8},{8,10},{10,12},{12,14},{14,16},{16,18},{18... | collective-permute-start | bytes 688136 | tf_op jit(solution)/shard_map/ppermute | solution.py:60
  40.0 11.2 %copy-start.13 = (bf16[256,128,1]{1,0,2:T(8,128)(2,1)S(1)}, bf16[256,128,1]{1,0,2:T(8,128)(2,1)}, u32[]{:S(2)}) copy-start(bf16[256,128,1]{1,0,2:T(8,128)(2,1)} %constant.65) | copy-start | bytes 196612
  40.1 10.7 %collective-permute-start.2 = (bf16[64,256]{1,0:T(8,128)(2,1)S(1)}, bf16[64,256]{1,0:T(8,128)(2,1)S(1)}, u32[]{:S(2)}, u32[]{:S(2)}) collective-permute-start(bf16[64,256]{1,0:T(8,128)(2,1)S(1)} %slice.370), channel_id=1, source_target_pairs={{0,4},{2,6},{4,8},{6,10},{8,12},{10,14},{12,16},{14,18},{16,20},{1... | collective-permute-start | bytes 98312 | tf_op jit(solution)/shard_map/ppermute | solution.py:60
  53.3 4.4 %copy-start.17 = (f32[1,512]{1,0:T(1,128)S(1)}, f32[1,512]{1,0:T(1,128)}, u32[]{:S(2)}) copy-start(f32[1,512]{1,0:T(1,128)} %get-tuple-element.33) | copy-start | bytes 6148
  53.3 4.4 %copy-start.18 = (f32[1,512]{1,0:T(1,128)S(1)}, f32[1,512]{1,0:T(1,128)}, u32[]{:S(2)}) copy-start(f32[1,512]{1,0:T(1,128)} %get-tuple-element.35) | copy-start | bytes 6148

commit v2 on v0

v2 whole, which is shorter than its diff:
```python
import functools

import jax
import jax.numpy as jnp
import numpy as np
from jax import lax
from jax.experimental import pallas as pl
from jax.experimental.pallas import tpu as pltpu
from jax.sharding import PartitionSpec as P

BLOCK = 128
CHUNK = 64
STRIP = 16
BF16 = jnp.bfloat16
F32 = jnp.float32
MESH = pl.DeviceIdType.MESH


def halves(matrix):
    high = matrix.astype(np.float32).astype(BF16)
    low = (matrix - high.astype(np.float64)).astype(np.float32).astype(BF16)
    return high, low


def spectra():
    odd = 2 * np.arange(BLOCK)[:, None] + 1
    angle = np.pi * odd * np.arange(BLOCK)[None, :] / (2 * BLOCK)
    forward = np.concatenate([np.cos(angle), -np.sin(angle)])
    reverse = forward[:, ::-1]
    angle = angle + np.pi * odd / 2
    inverse = np.concatenate([np.cos(angle), -np.sin(angle)]).T / BLOCK
    high, low = halves(inverse)
    return (
        np.concatenate(halves(forward), axis=1),
        np.concatenate(halves(reverse), axis=1),
        np.concatenate([high, high, low], axis=1),
    )


def kernel(
    devices,
    x_hbm, gain_hbm, wv_hbm, wg_hbm, taps_hbm, bias_hbm, cgain_hbm, cshift_hbm, wo_hbm, fwd_hbm, rev_hbm, inv_hbm,
    out_hbm,
    x, w, wo, taps, gain, bias, cgain, cshift, fwd, rev, inv,
    normed, own, halo, spec, lags, lag, prod, both, mixed, result,
    load_sem, send_sem, recv_sem, relay_send, relay_recv, pair_send, pair_recv, out_sem,
):
    tokens, width = x.shape
    layers = w.shape[0]
    half = w.shape[2] // 2
    chunks = tokens // CHUNK
    me, core = lax.axis_index("sp"), lax.axis_index("tp")
    after, before = lax.rem(me + 1, devices), lax.rem(me + devices - 1, devices)
    has_next, has_prev = me < devices - 1, me > 0

    barrier = pltpu.get_barrier_semaphore()
    pl.semaphore_signal(barrier, inc=1, device_id=(me, 1 - core), device_id_type=MESH)

    @pl.when(has_next)
    def _():
        pl.semaphore_signal(barrier, inc=1, device_id=(after, core), device_id_type=MESH)

    @pl.when(has_prev)
    def _():
        pl.semaphore_signal(barrier, inc=1, device_id=(before, core), device_id_type=MESH)

    loads = {}

    def load(name, source, target):
        loads[name] = pltpu.make_async_copy(source, target, load_sem.at[len(loads)])
        loads[name].start()

    def arrived(*names):
        for name in names:
            loads[name].wait()

    first = [(320, 448), (192, 320), (64, 192), (0, 64)]
    later = [(384, 448), (256, 384), (128, 256), (0, 128)]

    load("gain", gain_hbm, gain)
    load(("x", 0), x_hbm.at[pl.ds(320, 128)], x.at[pl.ds(320, 128)])
    load(("wv", 0), wv_hbm.at[0], w.at[0, :, pl.ds(0, half)])
    load(("wg", 0), wg_hbm.at[0], w.at[0, :, pl.ds(half, half)])
    for i in (1, 2, 3):
        rows = pl.ds(first[i][0], first[i][1] - first[i][0])
        load(("x", i), x_hbm.at[rows], x.at[rows])
    load("fwd", fwd_hbm, fwd)
    load("rev", rev_hbm, rev)
    load("taps", taps_hbm, taps)
    load("inv", inv_hbm, inv)
    load("bias", bias_hbm, bias)
    load("cgain", cgain_hbm, cgain)
    load("cshift", cshift_hbm, cshift)
    load(("wo", 0), wo_hbm.at[0], wo.at[0])
    load(("wv", 1), wv_hbm.at[1], w.at[1, :, pl.ds(0, half)])
    load(("wg", 1), wg_hbm.at[1], w.at[1, :, pl.ds(half, half)])
    load(("wo", 1), wo_hbm.at[1], wo.at[1])

    for layer in range(layers):
        own[layer, pl.ds(tokens, own.shape[1] - tokens), :] = jnp.zeros((own.shape[1] - tokens, half), BF16)

    @pl.when(me == 0)
    def _():
        halo[...] = jnp.zeros_like(halo)

    def chunk(layer, j):
        row = tokens - CHUNK * (j + 1)
        return pltpu.make_async_remote_copy(
            src_ref=own.at[layer, pl.ds(row, CHUNK)],
            dst_ref=halo.at[layer, pl.ds(CHUNK + row, CHUNK)],
            send_sem=send_sem.at[layer, j],
            recv_sem=recv_sem.at[layer, j],
            device_id=(after, core),
            device_id_type=MESH,
        )

    def relay(layer):
        return pltpu.make_async_remote_copy(
            src_ref=halo.at[layer, pl.ds(tokens, CHUNK)],
            dst_ref=halo.at[layer, pl.ds(0, CHUNK)],
            send_sem=relay_send.at[layer],
            recv_sem=relay_recv.at[layer],
            device_id=(after, core),
            device_id_type=MESH,
        )

    def pair(layer, m):
        low, high = later[3 - m]
        rows = pl.ds(low, high - low)
        return pltpu.make_async_remote_copy(
            src_ref=both.at[layer, core, rows],
            dst_ref=both.at[layer, core, rows],
            send_sem=pair_send.at[layer, m],
            recv_sem=pair_recv.at[layer, m],
            device_id=(me, 1 - core),
            device_id_type=MESH,
        )

    def strips(count, step):
        lax.fori_loop(0, count // STRIP, lambda i, c: (step(pl.multiple_of(i * STRIP, STRIP)), c)[1], 0, unroll=True)

    def project(layer, low, high):
        count = high - low

        def step(r):
            values = x[pl.ds(low + r, STRIP), :].astype(F32)
            scale = lax.rsqrt(jnp.sum(values * values, axis=-1, keepdims=True) * (1.0 / width) + 1e-06)
            normed[pl.ds(r, STRIP), :] = (values * scale * gain[pl.ds(layer, 1), :]).astype(BF16)

        strips(count, step)
        mm = jnp.dot(normed[pl.ds(0, count), :], w[layer], preferred_element_type=F32)
        own[layer, pl.ds(low, count), :] = (mm[:, :half] * jax.nn.sigmoid(mm[:, half:])).astype(BF16)

    def send(layer, low, high):
        @pl.when(has_next)
        def _():
            for j in range((tokens - high) // CHUNK, (tokens - low) // CHUNK):
                chunk(layer, j).start()

    def received(layer, *which):
        @pl.when(has_prev)
        def _():
            for j in which:
                if j < chunks:
                    chunk(layer, j).wait_recv()
                else:
                    relay(layer).wait_recv()

    def send_relay(layer):
        @pl.when(has_next)
        def _():
            relay(layer).start()

    def transform(layer, s):
        if s < 0:
            block = halo[layer, pl.ds(BLOCK * (s + 4), BLOCK), :]
        else:
            block = own[layer, pl.ds(BLOCK * s, BLOCK), :]
        spec[layer, s + 4] = jnp.dot(fwd[...], jnp.concatenate([block, block]), preferred_element_type=F32)

    def tap_spectra(layer):
        for b in range(4):
            block = taps[layer, pl.ds(BLOCK * (3 - b), BLOCK), :]
            lag[b] = jnp.dot(rev[...], jnp.concatenate([block, block]), preferred_element_type=F32)

        def step(i, carry):
            r = pl.multiple_of(i * STRIP, STRIP)
            odd = lax.rem(lax.broadcasted_iota(jnp.int32, (STRIP, half), 0), 2)
            sign = 1.0 - 2.0 * odd.astype(F32)
            re = [lag[b, pl.ds(r, STRIP), :] for b in range(4)]
            im = [lag[b, pl.ds(BLOCK + r, STRIP), :] for b in range(4)]
            for c in range(5):
                new_re, new_im = 0.0, 0.0
                if c < 4:
                    new_re, new_im = sign * im[c], -sign * re[c]
                if c > 0:
                    new_re, new_im = new_re + re[c - 1], new_im + im[c - 1]
                lags[layer, c, pl.ds(r, STRIP), :] = new_re
                lags[layer, c, pl.ds(BLOCK + r, STRIP), :] = new_im
            return carry

        lax.fori_loop(0, BLOCK // STRIP, step, 0, unroll=True)

    def convolve(layer, m):
        low, high = later[3 - m]

        def step(r):
            y_re, y_im = 0.0, 0.0
            for c in range(5):
                h_re, h_im = lags[layer, c, pl.ds(r, STRIP), :], lags[layer, c, pl.ds(BLOCK + r, STRIP), :]
                s = m - c + 4
                a_re, a_im = spec[layer, s, pl.ds(r, STRIP), :], spec[layer, s, pl.ds(BLOCK + r, STRIP), :]
                y_re = y_re + (h_re * a_re - h_im * a_im)
                y_im = y_im + (h_re * a_im + h_im * a_re)
            for at, y in ((0, y_re), (BLOCK, y_im)):
                top = y.astype(BF16)
                prod[pl.ds(at + r, STRIP), :] = top
                prod[pl.ds(2 * BLOCK + at + r, STRIP), :] = (y - top.astype(F32)).astype(BF16)
                prod[pl.ds(4 * BLOCK + at + r, STRIP), :] = top

        strips(BLOCK, step)
        conv = jnp.dot(inv[pl.ds(0, high - low), :], prod[...], preferred_element_type=F32)
        both[layer, core, pl.ds(low, high - low), :] = (conv + bias[pl.ds(layer, 1), :]).astype(BF16)
        pair(layer, m).start()

    def finish(layer, m):
        low, high = later[3 - m]
        count = high - low
        pair(layer, m).wait_recv()

        def step(r):
            parts = [both[layer, p, pl.ds(low + r, STRIP), :].astype(F32) for p in range(2)]
            center = sum(jnp.sum(v, axis=-1, keepdims=True) for v in parts) * (0.5 / half)
            parts = [v - center for v in parts]
            spread = sum(jnp.sum(v * v, axis=-1, keepdims=True) for v in parts) * (0.5 / half)
            scale = lax.rsqrt(spread + 1e-05)
            for p, v in enumerate(parts):
                columns = pl.ds(p * half, half)
                n = v * scale * cgain[pl.ds(layer, 1), columns] + cshift[pl.ds(layer, 1), columns]
                mixed[pl.ds(r, STRIP), columns] = (n * jax.nn.sigmoid(n)).astype(BF16)

        strips(count, step)
        rows = pl.ds(low, count)
        piece = 512
        target = x if layer < layers - 1 else result
        for at in range(0, width, piece):
            columns = pl.ds(at, piece)
            update = jnp.dot(mixed[pl.ds(0, count), :], wo[layer, :, columns], preferred_element_type=F32)
            target[rows, columns] = (x[rows, columns].astype(F32) + update).astype(BF16)

    def write(m):
        low, high = later[3 - m]
        rows = pl.ds(low, high - low)
        return pltpu.make_async_copy(result.at[rows], out_hbm.at[rows], out_sem.at[m])

    arrived("gain", ("x", 0))
    arrived(("wv", 0), ("wg", 0))
    project(0, *first[0])

    @pl.when(jnp.logical_and(has_prev, has_next))
    def _():
        pl.semaphore_wait(barrier, 3)

    @pl.when(jnp.logical_not(jnp.logical_and(has_prev, has_next)))
    def _():
        pl.semaphore_wait(barrier, 2)

    send(0, *first[0])
    for i in (1, 2, 3):
        arrived(("x", i))
        project(0, *first[i])
        send(0, *first[i])
    arrived("fwd", "rev", "taps", "inv", "bias", "cgain", "cshift")
    for s in (3, 2, 1, 0):
        transform(0, s)
    tap_spectra(0)
    tap_spectra(1)

    received(0, 0, 1)
    send_relay(0)
    transform(0, -1)
    convolve(0, 3)
    received(0, 2, 3)
    transform(0, -2)
    convolve(0, 2)
    arrived(("wo", 0), ("wv", 1), ("wg", 1))
    finish(0, 3)
    project(1, *later[0])
    send(1, *later[0])
    received(0, 4, 5)
    transform(0, -3)
    convolve(0, 1)
    finish(0, 2)
    project(1, *later[1])
    send(1, *later[1])
    received(0, 6, 7)
    transform(0, -4)
    convolve(0, 0)
    finish(0, 1)
    project(1, *later[2])
    send(1, *later[2])
    finish(0, 0)
    project(1, *later[3])
    send(1, *later[3])

    for s in (3, 2, 1, 0):
        transform(1, s)
    arrived(("wo", 1))
    received(1, 0, 1)
    send_relay(1)
    transform(1, -1)
    convolve(1, 3)
    received(1, 2, 3)
    transform(1, -2)
    convolve(1, 2)
    finish(1, 3)
    write(3).start()
    received(1, 4, 5)
    transform(1, -3)
    convolve(1, 1)
    finish(1, 2)
    write(2).start()
    received(1, 6, 7)
    transform(1, -4)
    convolve(1, 0)
    finish(1, 1)
    write(1).start()
    finish(1, 0)
    write(0).start()

    for layer in range(layers):
        for m in range(4):
            pair(layer, m).wait_send()

        @pl.when(has_next)
        def _():
            for j in range(chunks):
                chunk(layer, j).wait_send()
            relay(layer).wait_send()

    for m in range(4):
        write(m).wait()


def per_device(
    devices,
    stream,
    norm_gain,
    value_weight,
    gate_weight,
    conv_taps,
    conv_bias,
    channel_gain,
    channel_shift,
    out_weight,
):
    tokens, width = stream.shape
    layers, span, half = conv_taps.shape
    padded = -(-tokens // BLOCK) * BLOCK
    forward, reverse, inverse = (jnp.asarray(m) for m in spectra())
    dma = pltpu.SemaphoreType.DMA
    return pl.pallas_call(
        functools.partial(kernel, devices),
        out_shape=jax.ShapeDtypeStruct((tokens, width), BF16),
        in_specs=[pl.BlockSpec(memory_space=pl.ANY)] * 12,
        out_specs=pl.BlockSpec(memory_space=pl.ANY),
        scratch_shapes=[
            pltpu.VMEM((tokens, width), BF16),
            pltpu.VMEM((layers, width, 2 * half), BF16),
            pltpu.VMEM((layers, 2 * half, width), BF16),
            pltpu.VMEM((layers, span, half), BF16),
            pltpu.VMEM((layers, width), F32),
            pltpu.VMEM((layers, half), F32),
            pltpu.VMEM((layers, 2 * half), F32),
            pltpu.VMEM((layers, 2 * half), F32),
            pltpu.VMEM(forward.shape, BF16),
            pltpu.VMEM(reverse.shape, BF16),
            pltpu.VMEM(inverse.shape, BF16),
            pltpu.VMEM((BLOCK, width), BF16),
            pltpu.VMEM((layers, padded, half), BF16),
            pltpu.VMEM((layers, span, half), BF16),
            pltpu.VMEM((layers, 8, 2 * BLOCK, half), F32),
            pltpu.VMEM((layers, 5, 2 * BLOCK, half), F32),
            pltpu.VMEM((4, 2 * BLOCK, half), F32),
            pltpu.VMEM((6 * BLOCK, half), BF16),
            pltpu.VMEM((layers, 2, tokens, half), BF16),
            pltpu.VMEM((BLOCK, 2 * half), BF16),
            pltpu.VMEM((tokens, width), BF16),
            dma((24,)),
            dma((layers, tokens // CHUNK)),
            dma((layers, tokens // CHUNK)),
            dma((layers,)),
            dma((layers,)),
            dma((layers, 4)),
            dma((layers, 4)),
            dma((4,)),
        ],
        compiler_params=pltpu.CompilerParams(
            collective_id=0, has_side_effects=True, vmem_limit_bytes=60 * 1024 * 1024
        ),
        name="stacked_conv",
    )(
        stream, norm_gain, value_weight, gate_weight, conv_taps, conv_bias, channel_gain, channel_shift, out_weight,
        forward, reverse, inverse,
    )


def solution(mesh):
    return jax.shard_map(
        functools.partial(per_device, mesh.shape["sp"]),
        mesh=mesh,
        in_specs=(
            P("sp", None),
            P(),
            P(None, None, "tp"),
            P(None, None, "tp"),
            P(None, None, "tp"),
            P(None, "tp"),
            P(),
            P(),
            P(),
        ),
        out_specs=P("sp", None),
        check_vma=False,
    )
```

time: 103 us -> 30.1 us (0.29)
  the two profiles are of different devices: /device:TPU:129 before, /device:TPU:193 now
where the time goes in v2:
time: 30.1 us; the launch traced here: 30 us
  Pallas kernels  27 us (90%)
  local copies, waits for them, and re-layouts  2.94 us (10%)
    pallas_call x1, Pallas kernels, per_device(): pl.pallas_call(functools.partial(kernel, devices), out_shape=jax.ShapeDty...  27 us
    unnamed x1, local copies, waits for them, and re-layouts  2.94 us

profile of v2, /device:TPU:193, one launch (start us, length us, event | category | flops | bytes accessed | tf_op | source)
XLA Modules:
  0.0 30.0 jit_solution(704592391648585948)
XLA Ops:
  0.0 27.0 %stacked_conv.1 = bf16[448,2048]{1,0:T(8,128)(2,1)} custom-call(bf16[448,2048]{1,0:T(8,128)(2,1)} %x_hbm.1, f32[2,2048]{1,0:T(2,128)} %gain_hbm.1, bf16[2,2048,256]{2,1,0:T(8,128)(2,1)} %wv_hbm.1, bf16[2,2048,256]{2,1,0:T(8,128)(2,1)} %wg_hbm.1, bf16[2,512,256]{2,1,0:T(8,128)(2,1)} %taps_hbm.1, f32[2,256]{1,0:T(2,128)} %bias_hbm.1, f32[2,512]{1,0:T(2,128)} %cgain_hbm.1, ...), custom_call_target="tpu_custom_call" | custom-call | tf_op jit(solution)/shard_map/stacked_conv/pallas_call | solution.py:362
  27.0 2.9 %copy.14 = bf16[448,2048]{1,0:T(8,128)(2,1)} copy(bf16[448,2048]{1,0:T(8,128)(2,1)} %stacked_conv.1) | data formatting | bytes 3670016

commit v3 on v2

--- a/solution.py
+++ b/solution.py
@@ -13,7 +13,12 @@
 STRIP = 16
 BF16 = jnp.bfloat16
 F32 = jnp.float32
+LANES = 128
 MESH = pl.DeviceIdType.MESH
+
+
+def sigmoid(v):
+    return 0.5 * jnp.tanh(0.5 * v) + 0.5
 
 
 def halves(matrix):
@@ -40,10 +45,10 @@
 def kernel(
     devices,
     x_hbm, gain_hbm, wv_hbm, wg_hbm, taps_hbm, bias_hbm, cgain_hbm, cshift_hbm, wo_hbm, fwd_hbm, rev_hbm, inv_hbm,
-    out_hbm,
+    out,
     x, w, wo, taps, gain, bias, cgain, cshift, fwd, rev, inv,
-    normed, own, halo, spec, lags, lag, prod, both, mixed, result,
-    load_sem, send_sem, recv_sem, relay_send, relay_recv, pair_send, pair_recv, out_sem,
+    normed, own, halo, spec, lags, lag, prod, part, scales, both, mixed,
+    load_sem, send_sem, recv_sem, relay_send, relay_recv, pair_send, pair_recv,
 ):
     tokens, width = x.shape
     layers = w.shape[0]
@@ -56,20 +61,24 @@
     barrier = pltpu.get_barrier_semaphore()
     pl.semaphore_signal(barrier, inc=1, device_id=(me, 1 - core), device_id_type=MESH)
 
-    @pl.when(has_next)
-    def _():
-        pl.semaphore_signal(barrier, inc=1, device_id=(after, core), device_id_type=MESH)
-
     @pl.when(has_prev)
     def _():
         pl.semaphore_signal(barrier, inc=1, device_id=(before, core), device_id_type=MESH)
 
+    def scoped(f):
+        def inner(*a):
+            with jax.named_scope(f.__name__):
+                return f(*a)
+
+        return inner
+
     loads = {}
 
     def load(name, source, target):
         loads[name] = pltpu.make_async_copy(source, target, load_sem.at[len(loads)])
         loads[name].start()
 
+    @scoped
     def arrived(*names):
         for name in names:
             loads[name].wait()
@@ -139,17 +148,30 @@
     def strips(count, step):
         lax.fori_loop(0, count // STRIP, lambda i, c: (step(pl.multiple_of(i * STRIP, STRIP)), c)[1], 0, unroll=True)
 
-    def project(layer, low, high):
+    def gate(layer, low, count, scale):
+        mm = jnp.dot(normed[pl.ds(0, count), :], w[layer], preferred_element_type=F32)
+        values, gates = mm[:, :half] * scale, mm[:, half:] * scale
+        own[layer, pl.ds(low, count), :] = (values * sigmoid(gates)).astype(BF16)
+
+    def row_scale(squares):
+        return lax.rsqrt(jnp.sum(squares, axis=-1, keepdims=True) * (1.0 / width) + 1e-06)
+
+    @scoped
+    def prepare(low, high):
         count = high - low
 
         def step(r):
             values = x[pl.ds(low + r, STRIP), :].astype(F32)
-            scale = lax.rsqrt(jnp.sum(values * values, axis=-1, keepdims=True) * (1.0 / width) + 1e-06)
-            normed[pl.ds(r, STRIP), :] = (values * scale * gain[pl.ds(layer, 1), :]).astype(BF16)
+            normed[pl.ds(r, STRIP), :] = (values * gain[pl.ds(0, 1), :]).astype(BF16)
+            squares = sum(values[:, at : at + LANES] * values[:, at : at + LANES] for at in range(0, width, LANES))
+            scales[pl.ds(r, STRIP), :] = jnp.broadcast_to(row_scale(squares), (STRIP, LANES))
 
         strips(count, step)
-        mm = jnp.dot(normed[pl.ds(0, count), :], w[layer], preferred_element_type=F32)
-        own[layer, pl.ds(low, count), :] = (mm[:, :half] * jax.nn.sigmoid(mm[:, half:])).astype(BF16)
+
+    @scoped
+    def project(low, high):
+        scale = scales[pl.ds(0, high - low), :]
+        gate(0, low, high - low, jnp.concatenate([scale] * (half // LANES), axis=1))
 
     def send(layer, low, high):
         @pl.when(has_next)
@@ -157,6 +179,7 @@
             for j in range((tokens - high) // CHUNK, (tokens - low) // CHUNK):
                 chunk(layer, j).start()
 
+    @scoped
     def received(layer, *which):
         @pl.when(has_prev)
         def _():
@@ -171,6 +194,7 @@
         def _():
             relay(layer).start()
 
+    @scoped
     def transform(layer, s):
         if s < 0:
             block = halo[layer, pl.ds(BLOCK * (s + 4), BLOCK), :]
@@ -178,6 +202,7 @@
             block = own[layer, pl.ds(BLOCK * s, BLOCK), :]
         spec[layer, s + 4] = jnp.dot(fwd[...], jnp.concatenate([block, block]), preferred_element_type=F32)
 
+    @scoped
     def tap_spectra(layer):
         for b in range(4):
             block = taps[layer, pl.ds(BLOCK * (3 - b), BLOCK), :]
@@ -201,132 +226,150 @@
 
         lax.fori_loop(0, BLOCK // STRIP, step, 0, unroll=True)
 
-    def convolve(layer, m):
+    def products(layer, m, r, taken):
+        y_re, y_im = 0.0, 0.0
+        for c in taken:
+            h_re, h_im = lags[layer, c, pl.ds(r, STRIP), :], lags[layer, c, pl.ds(BLOCK + r, STRIP), :]
+            s = m - c + 4
+            a_re, a_im = spec[layer, s, pl.ds(r, STRIP), :], spec[layer, s, pl.ds(BLOCK + r, STRIP), :]
+            y_re = y_re + (h_re * a_re - h_im * a_im)
+            y_im = y_im + (h_re * a_im + h_im * a_re)
+        return y_re, y_im
+
+    @scoped
+    def own_part(layer, since):
+        for m in range(since, 4):
+
+            def step(r):
+                y_re, y_im = products(layer, m, r, range(m + 1 - since))
+                part[m, pl.ds(r, STRIP), :] = y_re
+                part[m, pl.ds(BLOCK + r, STRIP), :] = y_im
+
+            strips(BLOCK, step)
+
+    @scoped
+    def convolve(layer, m, since):
         low, high = later[3 - m]
 
         def step(r):
-            y_re, y_im = 0.0, 0.0
-            for c in range(5):
-                h_re, h_im = lags[layer, c, pl.ds(r, STRIP), :], lags[layer, c, pl.ds(BLOCK + r, STRIP), :]
-                s = m - c + 4
-                a_re, a_im = spec[layer, s, pl.ds(r, STRIP), :], spec[layer, s, pl.ds(BLOCK + r, STRIP), :]
-                y_re = y_re + (h_re * a_re - h_im * a_im)
-                y_im = y_im + (h_re * a_im + h_im * a_re)
+            y_re, y_im = products(layer, m, r, range(max(m + 1 - since, 0), 5))
+            if m >= since:
+                y_re, y_im = y_re + part[m, pl.ds(r, STRIP), :], y_im + part[m, pl.ds(BLOCK + r, STRIP), :]
             for at, y in ((0, y_re), (BLOCK, y_im)):
                 top = y.astype(BF16)
                 prod[pl.ds(at + r, STRIP), :] = top
                 prod[pl.ds(2 * BLOCK + at + r, STRIP), :] = (y - top.astype(F32)).astype(BF16)
-                prod[pl.ds(4 * BLOCK + at + r, STRIP), :] = top
 
         strips(BLOCK, step)
-        conv = jnp.dot(inv[pl.ds(0, high - low), :], prod[...], preferred_element_type=F32)
+        rows = pl.ds(0, high - low)
+        conv = jnp.dot(inv[rows, pl.ds(0, 4 * BLOCK)], prod[...], preferred_element_type=F32)
+        conv += jnp.dot(inv[rows, pl.ds(4 * BLOCK, 2 * BLOCK)], prod[pl.ds(0, 2 * BLOCK), :], preferred_element_type=F32)
         both[layer, core, pl.ds(low, high - low), :] = (conv + bias[pl.ds(layer, 1), :]).astype(BF16)
         pair(layer, m).start()
 
-    def finish(layer, m):
+    @scoped
+    def paired(layer, *which):
+        for m in which:
+            pair(layer, m).wait_recv()
+
+    @scoped
+    def mix(layer, m):
         low, high = later[3 - m]
-        count = high - low
-        pair(layer, m).wait_recv()
 
         def step(r):
-            parts = [both[layer, p, pl.ds(low + r, STRIP), :].astype(F32) for p in range(2)]
-            center = sum(jnp.sum(v, axis=-1, keepdims=True) for v in parts) * (0.5 / half)
+            rows = pl.ds(low + r, STRIP)
+            parts = [both[layer, p, rows, :].astype(F32) for p in range(2)]
+            center = jnp.sum(parts[0] + parts[1], axis=-1, keepdims=True) * (0.5 / half)
             parts = [v - center for v in parts]
-            spread = sum(jnp.sum(v * v, axis=-1, keepdims=True) for v in parts) * (0.5 / half)
+            spread = jnp.sum(parts[0] * parts[0] + parts[1] * parts[1], axis=-1, keepdims=True) * (0.5 / half)
             scale = lax.rsqrt(spread + 1e-05)
             for p, v in enumerate(parts):
                 columns = pl.ds(p * half, half)
                 n = v * scale * cgain[pl.ds(layer, 1), columns] + cshift[pl.ds(layer, 1), columns]
-                mixed[pl.ds(r, STRIP), columns] = (n * jax.nn.sigmoid(n)).astype(BF16)
-
-        strips(count, step)
+                mixed[rows, columns] = (n * sigmoid(n)).astype(BF16)
+
+        strips(high - low, step)
+
+    @scoped
+    def finish(layer, *which):
+        low, high = min(later[3 - m][0] for m in which), max(later[3 - m][1] for m in which)
+        count = high - low
         rows = pl.ds(low, count)
         piece = 512
-        target = x if layer < layers - 1 else result
+        squares = 0.0
         for at in range(0, width, piece):
             columns = pl.ds(at, piece)
-            update = jnp.dot(mixed[pl.ds(0, count), :], wo[layer, :, columns], preferred_element_type=F32)
-            target[rows, columns] = (x[rows, columns].astype(F32) + update).astype(BF16)
-
-    def write(m):
-        low, high = later[3 - m]
-        rows = pl.ds(low, high - low)
-        return pltpu.make_async_copy(result.at[rows], out_hbm.at[rows], out_sem.at[m])
+            update = jnp.dot(mixed[rows, :], wo[layer, :, columns], preferred_element_type=F32)
+            state = (x[rows, columns].astype(F32) + update).astype(BF16)
+            if layer == layers - 1:
+                out[rows, columns] = state
+                continue
+            x[rows, columns] = state
+            state = state.astype(F32)
+            normed[pl.ds(0, count), columns] = (state * gain[pl.ds(layer + 1, 1), columns]).astype(BF16)
+            squares = squares + sum(state[:, q : q + LANES] * state[:, q : q + LANES] for q in range(0, piece, LANES))
+        if layer < layers - 1:
+            gate(layer + 1, low, count, row_scale(squares))
+            send(layer + 1, low, high)
 
     arrived("gain", ("x", 0))
+    prepare(*first[0])
     arrived(("wv", 0), ("wg", 0))
-    project(0, *first[0])
-
-    @pl.when(jnp.logical_and(has_prev, has_next))
-    def _():
-        pl.semaphore_wait(barrier, 3)
-
-    @pl.when(jnp.logical_not(jnp.logical_and(has_prev, has_next)))
-    def _():
-        pl.semaphore_wait(barrier, 2)
+    project(*first[0])
+    with jax.named_scope("barrier"):
+
+        @pl.when(has_next)
+        def _():
+            pl.semaphore_wait(barrier, 2)
+
+        @pl.when(jnp.logical_not(has_next))
+        def _():
+            pl.semaphore_wait(barrier, 1)
 
     send(0, *first[0])
     for i in (1, 2, 3):
         arrived(("x", i))
-        project(0, *first[i])
+        prepare(*first[i])
+        project(*first[i])
         send(0, *first[i])
     arrived("fwd", "rev", "taps", "inv", "bias", "cgain", "cshift")
     for s in (3, 2, 1, 0):
         transform(0, s)
     tap_spectra(0)
+    own_part(0, 0)
     tap_spectra(1)
 
-    received(0, 0, 1)
-    send_relay(0)
-    transform(0, -1)
-    convolve(0, 3)
-    received(0, 2, 3)
-    transform(0, -2)
-    convolve(0, 2)
-    arrived(("wo", 0), ("wv", 1), ("wg", 1))
-    finish(0, 3)
-    project(1, *later[0])
-    send(1, *later[0])
-    received(0, 4, 5)
-    transform(0, -3)
-    convolve(0, 1)
-    finish(0, 2)
-    project(1, *later[1])
-    send(1, *later[1])
-    received(0, 6, 7)
-    transform(0, -4)
-    convolve(0, 0)
-    finish(0, 1)
-    project(1, *later[2])
-    send(1, *later[2])
-    finish(0, 0)
-    project(1, *later[3])
-    send(1, *later[3])
-
-    for s in (3, 2, 1, 0):
-        transform(1, s)
-    arrived(("wo", 1))
-    received(1, 0, 1)
-    send_relay(1)
-    transform(1, -1)
-    convolve(1, 3)
-    received(1, 2, 3)
-    transform(1, -2)
-    convolve(1, 2)
-    finish(1, 3)
-    write(3).start()
-    received(1, 4, 5)
-    transform(1, -3)
-    convolve(1, 1)
-    finish(1, 2)
-    write(2).start()
-    received(1, 6, 7)
-    transform(1, -4)
-    convolve(1, 0)
-    finish(1, 1)
-    write(1).start()
-    finish(1, 0)
-    write(0).start()
+    for layer, since in ((0, 0), (1, 1)):
+        received(layer, 0, 1)
+        send_relay(layer)
+        transform(layer, -1)
+        convolve(layer, 3, since)
+        received(layer, 2, 3)
+        transform(layer, -2)
+        convolve(layer, 2, since)
+        if layer == 0:
+            arrived(("wo", 0), ("wv", 1), ("wg", 1))
+        received(layer, 4, 5)
+        paired(layer, 3, 2)
+        transform(layer, -3)
+        convolve(layer, 1, since)
+        mix(layer, 3)
+        mix(layer, 2)
+        finish(layer, 3, 2)
+        received(layer, 6, 7)
+        transform(layer, -4)
+        convolve(layer, 0, since)
+        paired(layer, 1)
+        mix(layer, 1)
+        finish(layer, 1)
+        paired(layer, 0)
+        mix(layer, 0)
+        finish(layer, 0)
+        if layer == 0:
+            for s in (3, 2, 1, 0):
+                transform(1, s)
+            own_part(1, 1)
+            arrived(("wo", 1))
 
     for layer in range(layers):
         for m in range(4):
@@ -337,9 +380,6 @@
             for j in range(chunks):
                 chunk(layer, j).wait_send()
             relay(layer).wait_send()
-
-    for m in range(4):
-        write(m).wait()
 
 
 def per_device(
@@ -361,9 +401,9 @@
     dma = pltpu.SemaphoreType.DMA
     return pl.pallas_call(
         functools.partial(kernel, devices),
-        out_shape=jax.ShapeDtypeStruct((tokens, width), BF16),
-        in_specs=[pl.BlockSpec(memory_space=pl.ANY)] * 12,
-        out_specs=pl.BlockSpec(memory_space=pl.ANY),
+        out_shape=pltpu.VMEM((tokens, width), BF16),
+        in_specs=[pl.BlockSpec(memory_space=pltpu.HBM)] * 12,
+        out_specs=pl.BlockSpec(memory_space=pltpu.VMEM),
         scratch_shapes=[
             pltpu.VMEM((tokens, width), BF16),
             pltpu.VMEM((layers, width, 2 * half), BF16),
@@ -376,16 +416,17 @@
             pltpu.VMEM(forward.shape, BF16),
             pltpu.VMEM(reverse.shape, BF16),
             pltpu.VMEM(inverse.shape, BF16),
-            pltpu.VMEM((BLOCK, width), BF16),
+            pltpu.VMEM((2 * BLOCK, width), BF16),
             pltpu.VMEM((layers, padded, half), BF16),
             pltpu.VMEM((layers, span, half), BF16),
             pltpu.VMEM((layers, 8, 2 * BLOCK, half), F32),
             pltpu.VMEM((layers, 5, 2 * BLOCK, half), F32),
             pltpu.VMEM((4, 2 * BLOCK, half), F32),
-            pltpu.VMEM((6 * BLOCK, half), BF16),
+            pltpu.VMEM((4 * BLOCK, half), BF16),
+            pltpu.VMEM((4, 2 * BLOCK, half), F32),
+            pltpu.VMEM((BLOCK, LANES), F32),
             pltpu.VMEM((layers, 2, tokens, half), BF16),
-            pltpu.VMEM((BLOCK, 2 * half), BF16),
-            pltpu.VMEM((tokens, width), BF16),
+            pltpu.VMEM((tokens, 2 * half), BF16),
             dma((24,)),
             dma((layers, tokens // CHUNK)),
             dma((layers, tokens // CHUNK)),
@@ -393,7 +434,6 @@
             dma((layers,)),
             dma((layers, 4)),
             dma((layers, 4)),
-            dma((4,)),
         ],
         compiler_params=pltpu.CompilerParams(
             collective_id=0, has_side_effects=True, vmem_limit_bytes=60 * 1024 * 1024

time: 30.1 us -> 27.8 us (0.924)
  local copies, waits for them, and re-layouts: 2.94 us -> 1.23 us
  Pallas kernels: 27 us -> 26.4 us
    unnamed x1, local copies, waits for them, and re-layouts: 2.94 us -> 1.23 us
    pallas_call x1, Pallas kernels: 27 us -> 26.4 us  [per_device(): pl.pallas_call(functools.partial(kernel, devices), out_shape=pltpu.VMEM((...]
where the time goes in v3:
time: 27.8 us; the launch traced here: 27.7 us
  Pallas kernels  26.4 us (95%)
  local copies, waits for them, and re-layouts  1.23 us (4%)
    pallas_call x1, Pallas kernels, per_device(): pl.pallas_call(functools.partial(kernel, devices), out_shape=pltpu.VMEM((...  26.4 us
    unnamed x1, local copies, waits for them, and re-layouts  1.23 us

profile of v3, /device:TPU:193, one launch (start us, length us, event | category | flops | bytes accessed | tf_op | source)
XLA Modules:
  0.0 27.7 jit_solution(2374139883381711852)
XLA Ops:
  0.0 26.4 %stacked_conv.1 = bf16[448,2048]{1,0:T(8,128)(2,1)S(1)} custom-call(bf16[448,2048]{1,0:T(8,128)(2,1)} %x_hbm.1, f32[2,2048]{1,0:T(2,128)} %gain_hbm.1, bf16[2,2048,256]{2,1,0:T(8,128)(2,1)} %wv_hbm.1, bf16[2,2048,256]{2,1,0:T(8,128)(2,1)} %wg_hbm.1, bf16[2,512,256]{2,1,0:T(8,128)(2,1)} %taps_hbm.1, f32[2,256]{1,0:T(2,128)} %bias_hbm.1, f32[2,512]{1,0:T(2,128)} %cgain_hbm.1, ...), custom_call_target="tpu_custom_call" | custom-call | tf_op jit(solution)/shard_map/stacked_conv/pallas_call | solution.py:402
  26.5 1.2 %copy.14 = bf16[448,2048]{1,0:T(8,128)(2,1)} copy(bf16[448,2048]{1,0:T(8,128)(2,1)S(1)} %stacked_conv.1) | data formatting | bytes 3670016

commit v4 on v3

--- a/solution.py
+++ b/solution.py
@@ -14,6 +14,7 @@
 BF16 = jnp.bfloat16
 F32 = jnp.float32
 LANES = 128
+PIECES = 4
 MESH = pl.DeviceIdType.MESH
 
 
@@ -88,8 +89,10 @@
 
     load("gain", gain_hbm, gain)
     load(("x", 0), x_hbm.at[pl.ds(320, 128)], x.at[pl.ds(320, 128)])
-    load(("wv", 0), wv_hbm.at[0], w.at[0, :, pl.ds(0, half)])
-    load(("wg", 0), wg_hbm.at[0], w.at[0, :, pl.ds(half, half)])
+    for k in range(PIECES):
+        features = pl.ds(k * (width // PIECES), width // PIECES)
+        load(("wv", 0, k), wv_hbm.at[0, features], w.at[0, features, pl.ds(0, half)])
+        load(("wg", 0, k), wg_hbm.at[0, features], w.at[0, features, pl.ds(half, half)])
     for i in (1, 2, 3):
         rows = pl.ds(first[i][0], first[i][1] - first[i][0])
         load(("x", i), x_hbm.at[rows], x.at[rows])
@@ -148,8 +151,7 @@
     def strips(count, step):
         lax.fori_loop(0, count // STRIP, lambda i, c: (step(pl.multiple_of(i * STRIP, STRIP)), c)[1], 0, unroll=True)
 
-    def gate(layer, low, count, scale):
-        mm = jnp.dot(normed[pl.ds(0, count), :], w[layer], preferred_element_type=F32)
+    def gate(layer, low, count, scale, mm):
         values, gates = mm[:, :half] * scale, mm[:, half:] * scale
         own[layer, pl.ds(low, count), :] = (values * sigmoid(gates)).astype(BF16)
 
@@ -169,12 +171,19 @@
         strips(count, step)
 
     @scoped
-    def project(low, high):
-        scale = scales[pl.ds(0, high - low), :]
-        gate(0, low, high - low, jnp.concatenate([scale] * (half // LANES), axis=1))
-
-    def send(layer, low, high):
-        @pl.when(has_next)
+    def project(low, high, pieces=1):
+        count = high - low
+        mm = 0.0
+        for k in range(pieces):
+            if pieces > 1:
+                arrived(("wv", 0, k), ("wg", 0, k))
+            features = pl.ds(k * (width // pieces), width // pieces)
+            mm = mm + jnp.dot(normed[pl.ds(0, count), features], w[0, features, :], preferred_element_type=F32)
+        scale = scales[pl.ds(0, count), :]
+        gate(0, low, count, jnp.concatenate([scale] * (half // LANES), axis=1), mm)
+
+    def send(layer, low, high, who=None):
+        @pl.when(has_next if who is None else jnp.logical_and(has_next, core == who))
         def _():
             for j in range((tokens - high) // CHUNK, (tokens - low) // CHUNK):
                 chunk(layer, j).start()
@@ -237,24 +246,21 @@
         return y_re, y_im
 
     @scoped
-    def own_part(layer, since):
-        for m in range(since, 4):
-
-            def step(r):
-                y_re, y_im = products(layer, m, r, range(m + 1 - since))
-                part[m, pl.ds(r, STRIP), :] = y_re
-                part[m, pl.ds(BLOCK + r, STRIP), :] = y_im
-
-            strips(BLOCK, step)
-
-    @scoped
-    def convolve(layer, m, since):
+    def foresee(layer, m):
+        def step(r):
+            y_re, y_im = products(layer, m, r, range(4))
+            part[pl.ds(r, STRIP), :] = y_re
+            part[pl.ds(BLOCK + r, STRIP), :] = y_im
+
+        strips(BLOCK, step)
+
+    @scoped
+    def convolve(layer, m):
         low, high = later[3 - m]
 
         def step(r):
-            y_re, y_im = products(layer, m, r, range(max(m + 1 - since, 0), 5))
-            if m >= since:
-                y_re, y_im = y_re + part[m, pl.ds(r, STRIP), :], y_im + part[m, pl.ds(BLOCK + r, STRIP), :]
+            y_re, y_im = products(layer, m, r, (4,))
+            y_re, y_im = y_re + part[pl.ds(r, STRIP), :], y_im + part[pl.ds(BLOCK + r, STRIP), :]
             for at, y in ((0, y_re), (BLOCK, y_im)):
                 top = y.astype(BF16)
                 prod[pl.ds(at + r, STRIP), :] = top
@@ -296,26 +302,33 @@
         count = high - low
         rows = pl.ds(low, count)
         piece = 512
-        squares = 0.0
+        squares, mm, ahead = 0.0, 0.0, None
+
+        def widen(at):
+            return jnp.dot(mixed[rows, :], wo[layer, :, pl.ds(at, piece)], preferred_element_type=F32)
+
+        update = widen(0)
         for at in range(0, width, piece):
             columns = pl.ds(at, piece)
-            update = jnp.dot(mixed[rows, :], wo[layer, :, columns], preferred_element_type=F32)
+            if at + piece < width:
+                ahead = widen(at + piece)
             state = (x[rows, columns].astype(F32) + update).astype(BF16)
+            update = ahead
             if layer == layers - 1:
                 out[rows, columns] = state
                 continue
             x[rows, columns] = state
             state = state.astype(F32)
-            normed[pl.ds(0, count), columns] = (state * gain[pl.ds(layer + 1, 1), columns]).astype(BF16)
+            scaled = (state * gain[pl.ds(layer + 1, 1), columns]).astype(BF16)
+            mm = mm + jnp.dot(scaled, w[layer + 1, columns, :], preferred_element_type=F32)
             squares = squares + sum(state[:, q : q + LANES] * state[:, q : q + LANES] for q in range(0, piece, LANES))
         if layer < layers - 1:
-            gate(layer + 1, low, count, row_scale(squares))
+            gate(layer + 1, low, count, row_scale(squares), mm)
             send(layer + 1, low, high)
 
     arrived("gain", ("x", 0))
     prepare(*first[0])
-    arrived(("wv", 0), ("wg", 0))
-    project(*first[0])
+    project(*first[0], PIECES)
     with jax.named_scope("barrier"):
 
         @pl.when(has_next)
@@ -336,39 +349,48 @@
     for s in (3, 2, 1, 0):
         transform(0, s)
     tap_spectra(0)
-    own_part(0, 0)
+    foresee(0, 3)
     tap_spectra(1)
 
-    for layer, since in ((0, 0), (1, 1)):
+    for layer in range(layers):
         received(layer, 0, 1)
         send_relay(layer)
         transform(layer, -1)
-        convolve(layer, 3, since)
+        convolve(layer, 3)
+        foresee(layer, 2)
         received(layer, 2, 3)
         transform(layer, -2)
-        convolve(layer, 2, since)
+        convolve(layer, 2)
         if layer == 0:
             arrived(("wo", 0), ("wv", 1), ("wg", 1))
+        paired(layer, 3)
+        mix(layer, 3)
+        foresee(layer, 1)
+        finish(layer, 3)
         received(layer, 4, 5)
-        paired(layer, 3, 2)
         transform(layer, -3)
-        convolve(layer, 1, since)
-        mix(layer, 3)
+        convolve(layer, 1)
+        paired(layer, 2)
         mix(layer, 2)
-        finish(layer, 3, 2)
+        foresee(layer, 0)
+        finish(layer, 2)
         received(layer, 6, 7)
         transform(layer, -4)
-        convolve(layer, 0, since)
+        convolve(layer, 0)
         paired(layer, 1)
         mix(layer, 1)
+        if layer == 0:
+            transform(1, 3)
+            transform(1, 2)
         finish(layer, 1)
         paired(layer, 0)
         mix(layer, 0)
+        if layer == 0:
+            transform(1, 1)
         finish(layer, 0)
         if layer == 0:
-            for s in (3, 2, 1, 0):
-                transform(1, s)
-            own_part(1, 1)
+            transform(1, 0)
+            foresee(1, 3)
             arrived(("wo", 1))
 
     for layer in range(layers):
@@ -423,11 +445,11 @@
             pltpu.VMEM((layers, 5, 2 * BLOCK, half), F32),
             pltpu.VMEM((4, 2 * BLOCK, half), F32),
             pltpu.VMEM((4 * BLOCK, half), BF16),
-            pltpu.VMEM((4, 2 * BLOCK, half), F32),
+            pltpu.VMEM((2 * BLOCK, half), F32),
             pltpu.VMEM((BLOCK, LANES), F32),
             pltpu.VMEM((layers, 2, tokens, half), BF16),
             pltpu.VMEM((tokens, 2 * half), BF16),
-            dma((24,)),
+            dma((32,)),
             dma((layers, tokens // CHUNK)),
             dma((layers, tokens // CHUNK)),
             dma((layers,)),

time: 27.8 us -> 26.5 us (0.953)
  Pallas kernels: 26.4 us -> 25.1 us
    pallas_call x1, Pallas kernels: 26.4 us -> 25.1 us  [per_device(): pl.pallas_call(functools.partial(kernel, devices), out_shape=pltpu.VMEM((...]
where the time goes in v4:
time: 26.5 us; the launch traced here: 26.4 us
  Pallas kernels  25.1 us (95%)
  local copies, waits for them, and re-layouts  1.23 us (5%)
    pallas_call x1, Pallas kernels, per_device(): pl.pallas_call(functools.partial(kernel, devices), out_shape=pltpu.VMEM((...  25.1 us
    unnamed x1, local copies, waits for them, and re-layouts  1.23 us

profile of v4, /device:TPU:193, one launch (start us, length us, event | category | flops | bytes accessed | tf_op | source)
XLA Modules:
  0.0 26.4 jit_solution(13545570977366810385)
XLA Ops:
  0.0 25.1 %stacked_conv.1 = bf16[448,2048]{1,0:T(8,128)(2,1)S(1)} custom-call(bf16[448,2048]{1,0:T(8,128)(2,1)} %x_hbm.1, f32[2,2048]{1,0:T(2,128)} %gain_hbm.1, bf16[2,2048,256]{2,1,0:T(8,128)(2,1)} %wv_hbm.1, bf16[2,2048,256]{2,1,0:T(8,128)(2,1)} %wg_hbm.1, bf16[2,512,256]{2,1,0:T(8,128)(2,1)} %taps_hbm.1, f32[2,256]{1,0:T(2,128)} %bias_hbm.1, f32[2,512]{1,0:T(2,128)} %cgain_hbm.1, ...), custom_call_target="tpu_custom_call" | custom-call | tf_op jit(solution)/shard_map/stacked_conv/pallas_call | solution.py:424
  25.1 1.2 %copy.14 = bf16[448,2048]{1,0:T(8,128)(2,1)} copy(bf16[448,2048]{1,0:T(8,128)(2,1)S(1)} %stacked_conv.1) | data formatting | bytes 3670016

commit v5 on v4

--- a/solution.py
+++ b/solution.py
@@ -203,7 +203,6 @@
         def _():
             relay(layer).start()
 
-    @scoped
     def transform(layer, s):
         if s < 0:
             block = halo[layer, pl.ds(BLOCK * (s + 4), BLOCK), :]
@@ -245,22 +244,20 @@
             y_im = y_im + (h_re * a_im + h_im * a_re)
         return y_re, y_im
 
-    @scoped
     def foresee(layer, m):
         def step(r):
             y_re, y_im = products(layer, m, r, range(4))
-            part[pl.ds(r, STRIP), :] = y_re
-            part[pl.ds(BLOCK + r, STRIP), :] = y_im
+            part[m % 2, pl.ds(r, STRIP), :] = y_re
+            part[m % 2, pl.ds(BLOCK + r, STRIP), :] = y_im
 
         strips(BLOCK, step)
 
-    @scoped
     def convolve(layer, m):
         low, high = later[3 - m]
 
         def step(r):
             y_re, y_im = products(layer, m, r, (4,))
-            y_re, y_im = y_re + part[pl.ds(r, STRIP), :], y_im + part[pl.ds(BLOCK + r, STRIP), :]
+            y_re, y_im = y_re + part[m % 2, pl.ds(r, STRIP), :], y_im + part[m % 2, pl.ds(BLOCK + r, STRIP), :]
             for at, y in ((0, y_re), (BLOCK, y_im)):
                 top = y.astype(BF16)
                 prod[pl.ds(at + r, STRIP), :] = top
@@ -271,14 +268,12 @@
         conv = jnp.dot(inv[rows, pl.ds(0, 4 * BLOCK)], prod[...], preferred_element_type=F32)
         conv += jnp.dot(inv[rows, pl.ds(4 * BLOCK, 2 * BLOCK)], prod[pl.ds(0, 2 * BLOCK), :], preferred_element_type=F32)
         both[layer, core, pl.ds(low, high - low), :] = (conv + bias[pl.ds(layer, 1), :]).astype(BF16)
-        pair(layer, m).start()
 
     @scoped
     def paired(layer, *which):
         for m in which:
             pair(layer, m).wait_recv()
 
-    @scoped
     def mix(layer, m):
         low, high = later[3 - m]
 
@@ -326,6 +321,21 @@
             gate(layer + 1, low, count, row_scale(squares), mm)
             send(layer + 1, low, high)
 
+    @scoped
+    def step(layer, m):
+        transform(layer, m - 4)
+        convolve(layer, m)
+        if m > 0:
+            foresee(layer, m - 1)
+        pair(layer, m).start()
+
+    @scoped
+    def last(layer):
+        mix(layer, 0)
+        if layer == 0:
+            transform(1, 1)
+        finish(layer, 0)
+
     arrived("gain", ("x", 0))
     prepare(*first[0])
     project(*first[0], PIECES)
@@ -355,28 +365,25 @@
     for layer in range(layers):
         received(layer, 0, 1)
         send_relay(layer)
-        transform(layer, -1)
-        convolve(layer, 3)
-        foresee(layer, 2)
+        step(layer, 3)
         received(layer, 2, 3)
-        transform(layer, -2)
-        convolve(layer, 2)
+        step(layer, 2)
         if layer == 0:
             arrived(("wo", 0), ("wv", 1), ("wg", 1))
         paired(layer, 3)
         mix(layer, 3)
-        foresee(layer, 1)
         finish(layer, 3)
         received(layer, 4, 5)
-        transform(layer, -3)
-        convolve(layer, 1)
+        step(layer, 1)
+        if layer == layers - 1:
+            received(layer, 6, 7)
+            step(layer, 0)
         paired(layer, 2)
         mix(layer, 2)
-        foresee(layer, 0)
         finish(layer, 2)
-        received(layer, 6, 7)
-        transform(layer, -4)
-        convolve(layer, 0)
+        if layer < layers - 1:
+            received(layer, 6, 7)
+            step(layer, 0)
         paired(layer, 1)
         mix(layer, 1)
         if layer == 0:
@@ -384,10 +391,7 @@
             transform(1, 2)
         finish(layer, 1)
         paired(layer, 0)
-        mix(layer, 0)
-        if layer == 0:
-            transform(1, 1)
-        finish(layer, 0)
+        last(layer)
         if layer == 0:
             transform(1, 0)
             foresee(1, 3)
@@ -445,7 +449,7 @@
             pltpu.VMEM((layers, 5, 2 * BLOCK, half), F32),
             pltpu.VMEM((4, 2 * BLOCK, half), F32),
             pltpu.VMEM((4 * BLOCK, half), BF16),
-            pltpu.VMEM((2 * BLOCK, half), F32),
+            pltpu.VMEM((2, 2 * BLOCK, half), F32),
             pltpu.VMEM((BLOCK, LANES), F32),
             pltpu.VMEM((layers, 2, tokens, half), BF16),
             pltpu.VMEM((tokens, 2 * half), BF16),

time: 26.5 us -> 26.4 us (level)
  no operation moved by 1% of the time
where the time goes in v5:
time: 26.4 us; the launch traced here: 26.2 us
  Pallas kernels  25 us (95%)
  local copies, waits for them, and re-layouts  1.23 us (5%)
    pallas_call x1, Pallas kernels, per_device(): pl.pallas_call(functools.partial(kernel, devices), out_shape=pltpu.VMEM((...  25 us
    unnamed x1, local copies, waits for them, and re-layouts  1.23 us

profile of v5, /device:TPU:193, one launch (start us, length us, event | category | flops | bytes accessed | tf_op | source)
XLA Modules:
  0.0 26.2 jit_solution(9382200645092911638)
XLA Ops:
  0.0 25.0 %stacked_conv.1 = bf16[448,2048]{1,0:T(8,128)(2,1)S(1)} custom-call(bf16[448,2048]{1,0:T(8,128)(2,1)} %x_hbm.1, f32[2,2048]{1,0:T(2,128)} %gain_hbm.1, bf16[2,2048,256]{2,1,0:T(8,128)(2,1)} %wv_hbm.1, bf16[2,2048,256]{2,1,0:T(8,128)(2,1)} %wg_hbm.1, bf16[2,512,256]{2,1,0:T(8,128)(2,1)} %taps_hbm.1, f32[2,256]{1,0:T(2,128)} %bias_hbm.1, f32[2,512]{1,0:T(2,128)} %cgain_hbm.1, ...), custom_call_target="tpu_custom_call" | custom-call | tf_op jit(solution)/shard_map/stacked_conv/pallas_call | solution.py:428
  25.0 1.2 %copy.14 = bf16[448,2048]{1,0:T(8,128)(2,1)} copy(bf16[448,2048]{1,0:T(8,128)(2,1)S(1)} %stacked_conv.1) | data formatting | bytes 3670016

commit v6 on v5

--- a/solution.py
+++ b/solution.py
@@ -46,7 +46,7 @@
 def kernel(
     devices,
     x_hbm, gain_hbm, wv_hbm, wg_hbm, taps_hbm, bias_hbm, cgain_hbm, cshift_hbm, wo_hbm, fwd_hbm, rev_hbm, inv_hbm,
-    out,
+    out, mixed_out, wo_out,
     x, w, wo, taps, gain, bias, cgain, cshift, fwd, rev, inv,
     normed, own, halo, spec, lags, lag, prod, part, scales, both, mixed,
     load_sem, send_sem, recv_sem, relay_send, relay_recv, pair_send, pair_recv,
@@ -103,10 +103,10 @@
     load("bias", bias_hbm, bias)
     load("cgain", cgain_hbm, cgain)
     load("cshift", cshift_hbm, cshift)
-    load(("wo", 0), wo_hbm.at[0], wo.at[0])
+    load(("wo", 0), wo_hbm.at[0], wo)
     load(("wv", 1), wv_hbm.at[1], w.at[1, :, pl.ds(0, half)])
     load(("wg", 1), wg_hbm.at[1], w.at[1, :, pl.ds(half, half)])
-    load(("wo", 1), wo_hbm.at[1], wo.at[1])
+    load(("wo", 1), wo_hbm.at[1], wo_out)
 
     for layer in range(layers):
         own[layer, pl.ds(tokens, own.shape[1] - tokens), :] = jnp.zeros((own.shape[1] - tokens, half), BF16)
@@ -276,6 +276,7 @@
 
     def mix(layer, m):
         low, high = later[3 - m]
+        target = mixed_out if layer == layers - 1 and m == 0 else mixed
 
         def step(r):
             rows = pl.ds(low + r, STRIP)
@@ -287,7 +288,7 @@
             for p, v in enumerate(parts):
                 columns = pl.ds(p * half, half)
                 n = v * scale * cgain[pl.ds(layer, 1), columns] + cshift[pl.ds(layer, 1), columns]
-                mixed[rows, columns] = (n * sigmoid(n)).astype(BF16)
+                target[rows, columns] = (n * sigmoid(n)).astype(BF16)
 
         strips(high - low, step)
 
@@ -300,7 +301,7 @@
         squares, mm, ahead = 0.0, 0.0, None
 
         def widen(at):
-            return jnp.dot(mixed[rows, :], wo[layer, :, pl.ds(at, piece)], preferred_element_type=F32)
+            return jnp.dot(mixed[rows, :], (wo, wo_out)[layer][:, pl.ds(at, piece)], preferred_element_type=F32)
 
         update = widen(0)
         for at in range(0, width, piece):
@@ -313,6 +314,8 @@
                 out[rows, columns] = state
                 continue
             x[rows, columns] = state
+            if low == 0:
+                out[rows, columns] = state
             state = state.astype(F32)
             scaled = (state * gain[pl.ds(layer + 1, 1), columns]).astype(BF16)
             mm = mm + jnp.dot(scaled, w[layer + 1, columns, :], preferred_element_type=F32)
@@ -334,7 +337,8 @@
         mix(layer, 0)
         if layer == 0:
             transform(1, 1)
-        finish(layer, 0)
+        if layer < layers - 1:
+            finish(layer, 0)
 
     arrived("gain", ("x", 0))
     prepare(*first[0])
@@ -408,6 +412,25 @@
             relay(layer).wait_send()
 
 
+def close(result, mixed, wo, out_hbm, block, sem):
+    tokens, width = result.shape
+    count = mixed.shape[0]
+    rest = pl.ds(count, tokens - count)
+    copies = [pltpu.make_async_copy(result.at[rest], out_hbm.at[rest], sem.at[0])]
+    copies[0].start()
+    piece = 512
+    for i, at in enumerate(range(0, width, piece)):
+        columns = pl.ds(at, piece)
+        update = jnp.dot(mixed[...], wo[:, columns], preferred_element_type=F32)
+        block[:, columns] = (result[pl.ds(0, count), columns].astype(F32) + update).astype(BF16)
+        copies.append(
+            pltpu.make_async_copy(block.at[:, columns], out_hbm.at[pl.ds(0, count), columns], sem.at[1 + i])
+        )
+        copies[-1].start()
+    for copy in copies:
+        copy.wait()
+
+
 def per_device(
     devices,
     stream,
@@ -425,15 +448,19 @@
     padded = -(-tokens // BLOCK) * BLOCK
     forward, reverse, inverse = (jnp.asarray(m) for m in spectra())
     dma = pltpu.SemaphoreType.DMA
-    return pl.pallas_call(
+    result, mixed, wo = pl.pallas_call(
         functools.partial(kernel, devices),
-        out_shape=pltpu.VMEM((tokens, width), BF16),
+        out_shape=(
+            pltpu.VMEM((tokens, width), BF16),
+            pltpu.VMEM((BLOCK, 2 * half), BF16),
+            pltpu.VMEM((2 * half, width), BF16),
+        ),
         in_specs=[pl.BlockSpec(memory_space=pltpu.HBM)] * 12,
-        out_specs=pl.BlockSpec(memory_space=pltpu.VMEM),
+        out_specs=[pl.BlockSpec(memory_space=pltpu.VMEM)] * 3,
         scratch_shapes=[
             pltpu.VMEM((tokens, width), BF16),
             pltpu.VMEM((layers, width, 2 * half), BF16),
-            pltpu.VMEM((layers, 2 * half, width), BF16),
+            pltpu.VMEM((2 * half, width), BF16),
             pltpu.VMEM((layers, span, half), BF16),
             pltpu.VMEM((layers, width), F32),
             pltpu.VMEM((layers, half), F32),
@@ -462,13 +489,22 @@
             dma((layers, 4)),
         ],
         compiler_params=pltpu.CompilerParams(
-            collective_id=0, has_side_effects=True, vmem_limit_bytes=60 * 1024 * 1024
+            collective_id=0, has_side_effects=True, vmem_limit_bytes=59 * 1024 * 1024
         ),
         name="stacked_conv",
     )(
         stream, norm_gain, value_weight, gate_weight, conv_taps, conv_bias, channel_gain, channel_shift, out_weight,
         forward, reverse, inverse,
     )
+    return pl.pallas_call(
+        close,
+        out_shape=jax.ShapeDtypeStruct((tokens, width), BF16),
+        in_specs=[pl.BlockSpec(memory_space=pltpu.VMEM)] * 3,
+        out_specs=pl.BlockSpec(memory_space=pl.ANY),
+        scratch_shapes=[pltpu.VMEM((BLOCK, width), BF16), dma((5,))],
+        compiler_params=pltpu.CompilerParams(vmem_limit_bytes=16 * 1024 * 1024),
+        name="close",
+    )(result, mixed, wo)
 
 
 def solution(mesh):

time: 26.4 us -> 26 us (0.985)
  local copies, waits for them, and re-layouts: 1.23 us -> 0 us
  Pallas kernels: 25 us -> 25.9 us
    unnamed x1 -> x0, local copies, waits for them, and re-layouts: 1.23 us -> none
    pallas_call x1 -> x2, Pallas kernels: 25 us -> 25.9 us  [the longest x1 24.6 us: per_device(): pl.pallas_call(functools.partial(kernel, devices), out_shape=(pltpu.VMEM(...]
where the time goes in v6:
time: 26 us; the launch traced here: 25.9 us
  Pallas kernels  25.9 us (100%)
    pallas_call x1, Pallas kernels, per_device(): pl.pallas_call(functools.partial(kernel, devices), out_shape=(pltpu.VMEM(...  24.6 us
    pallas_call x1, Pallas kernels, per_device(): pl.pallas_call(close, out_shape=jax.ShapeDtypeStruct((tokens, width), BF1...  1.26 us

profile of v6, /device:TPU:193, one launch (start us, length us, event | category | flops | bytes accessed | tf_op | source)
XLA Modules:
  0.0 25.9 jit_solution(9663834778173885222)
XLA Ops:
  0.0 24.6 %stacked_conv.1 = (bf16[448,2048]{1,0:T(8,128)(2,1)S(1)}, bf16[128,512]{1,0:T(8,128)(2,1)S(1)}, bf16[512,2048]{1,0:T(8,128)(2,1)S(1)}) custom-call(bf16[448,2048]{1,0:T(8,128)(2,1)} %x_hbm.1, f32[2,2048]{1,0:T(2,128)} %gain_hbm.1, bf16[2,2048,256]{2,1,0:T(8,128)(2,1)} %wv_hbm.1, bf16[2,2048,256]{2,1,0:T(8,128)(2,1)} %wg_hbm.1, ...), custom_call_target="tpu_custom_call" | custom-call | tf_op jit(solution)/shard_map/stacked_conv/pallas_call | solution.py:451
  24.6 1.3 %close.1 = bf16[448,2048]{1,0:T(8,128)(2,1)} custom-call(bf16[448,2048]{1,0:T(8,128)(2,1)S(1)} %get-tuple-element.8.result, bf16[128,512]{1,0:T(8,128)(2,1)S(1)} %get-tuple-element.9.mixed, bf16[512,2048]{1,0:T(8,128)(2,1)S(1)} %get-tuple-element.10.wo), custom_call_target="tpu_custom_call" | custom-call | tf_op jit(solution)/shard_map/close/pallas_call | solution.py:499

commit v7 on v6

--- a/solution.py
+++ b/solution.py
@@ -14,7 +14,7 @@
 BF16 = jnp.bfloat16
 F32 = jnp.float32
 LANES = 128
-PIECES = 4
+PIECES = 8
 MESH = pl.DeviceIdType.MESH
 
 
@@ -208,7 +208,10 @@
             block = halo[layer, pl.ds(BLOCK * (s + 4), BLOCK), :]
         else:
             block = own[layer, pl.ds(BLOCK * s, BLOCK), :]
-        spec[layer, s + 4] = jnp.dot(fwd[...], jnp.concatenate([block, block]), preferred_element_type=F32)
+        twice = jnp.concatenate([block, block])
+        for at in (0, BLOCK):
+            rows = pl.ds(at, BLOCK)
+            spec[layer, s + 4, rows, :] = jnp.dot(fwd[rows, :], twice, preferred_element_type=F32)
 
     @scoped
     def tap_spectra(layer):

time: 26 us -> 26.2 us (level)
  no operation moved by 1% of the time
where the time goes in v7:
time: 26.2 us; the launch traced here: 26.1 us
  Pallas kernels  26 us (99%)
    pallas_call x1, Pallas kernels, per_device(): pl.pallas_call(functools.partial(kernel, devices), out_shape=(pltpu.VMEM(...  24.8 us
    pallas_call x1, Pallas kernels, per_device(): pl.pallas_call(close, out_shape=jax.ShapeDtypeStruct((tokens, width), BF1...  1.26 us

profile of v7, /device:TPU:193, one launch (start us, length us, event | category | flops | bytes accessed | tf_op | source)
XLA Modules:
  0.0 26.1 jit_solution(8012525977719313294)
XLA Ops:
  0.0 24.8 %stacked_conv.1 = (bf16[448,2048]{1,0:T(8,128)(2,1)S(1)}, bf16[128,512]{1,0:T(8,128)(2,1)S(1)}, bf16[512,2048]{1,0:T(8,128)(2,1)S(1)}) custom-call(bf16[448,2048]{1,0:T(8,128)(2,1)} %x_hbm.1, f32[2,2048]{1,0:T(2,128)} %gain_hbm.1, bf16[2,2048,256]{2,1,0:T(8,128)(2,1)} %wv_hbm.1, bf16[2,2048,256]{2,1,0:T(8,128)(2,1)} %wg_hbm.1, ...), custom_call_target="tpu_custom_call" | custom-call | tf_op jit(solution)/shard_map/stacked_conv/pallas_call | solution.py:454
  24.8 1.3 %close.1 = bf16[448,2048]{1,0:T(8,128)(2,1)} custom-call(bf16[448,2048]{1,0:T(8,128)(2,1)S(1)} %get-tuple-element.8.result, bf16[128,512]{1,0:T(8,128)(2,1)S(1)} %get-tuple-element.9.mixed, bf16[512,2048]{1,0:T(8,128)(2,1)S(1)} %get-tuple-element.10.wo), custom_call_target="tpu_custom_call" | custom-call | tf_op jit(solution)/shard_map/close/pallas_call | solution.py:502
